TPU v7x, 128 devices: a whole 4x4x4 slice. The times are simulated.
128 devices in a mesh: sp: 16 (over z, x), tp: 8 (over y, core).
Axes of the slice: x: 4, y: 4, z: 4, core: 2. Of those that a mesh axis runs over, the one named last changes fastest.
Arguments:
- hidden_states: bfloat16 [12288, 4096], P('sp'), may hold values from -60 to 60
- w_conv_b: bfloat16 [4096, 2048], P(None, 'tp'), may hold values from -0.09375 to 0.09375
- w_conv_c: bfloat16 [4096, 2048], P(None, 'tp'), may hold values from -0.09375 to 0.09375
- w_conv_h: bfloat16 [4096, 2048], P(None, 'tp'), may hold values from -0.09375 to 0.09375
- conv_taps: bfloat16 [3, 2048], P(None, 'tp'), may hold values from -3.5 to 3.5
- w_query: bfloat16 [4096, 2048], P(None, 'tp'), may hold values from -0.15625 to 0.15625
- w_key: bfloat16 [4096, 2048], P(None, 'tp'), may hold values from -0.09375 to 0.09375
- w_value: bfloat16 [4096, 2048], P(None, 'tp'), may hold values from -0.09375 to 0.09375
- lambdas: float32 [16], P('tp'), may hold values from 0.3 to 0.8
- head_gain: bfloat16 [128], replicated, may hold values from 0.099609375 to 1.8984375
- w_out_conv: bfloat16 [2048, 4096], P('tp'), may hold values from -1 to 1
- w_out_attn: bfloat16 [2048, 4096], P('tp'), may hold values from -1 to 1
- out_gain: bfloat16 [4096], replicated, may hold values from 0.099609375 to 1.8984375
Outputs:
- mixed: bfloat16 [12288, 4096], P('sp', 'tp')
All inputs are finite; a program needn't handle non-finite values.
Results may differ from a plain program's by a relative error of at most 0.023.
Values may be sent and summed in bfloat16 or wider, within the bound.
A program may use at most 192 MiB of HBM per device.

v0:
```python
import jax
import jax.numpy as jnp
from jax import lax
from jax.sharding import PartitionSpec as P

D = 4096
QK = 64
TAPS = 3
VD = 128


NEG_LARGE = -1e30


def sent_together(arrays, axis, dim, along):
    both = jnp.concatenate(arrays, axis=along)
    filled, at, finished = (lax.all_gather(both, axis, axis=dim, tiled=True), 0, [])
    for a in arrays:
        finished.append(lax.slice_in_dim(filled, at, at + a.shape[along], axis=along))
        at += a.shape[along]
    return tuple(finished)


def passed_along(block, axis, distance):
    devices = range(lax.axis_size(axis))
    route = [(i - distance, i) for i in devices if i - distance in devices]
    return lax.ppermute(block, axis, route)


def copy_for_each(value, axis):
    copies = jnp.broadcast_to(value, (lax.axis_size(axis), *value.shape))
    return lax.all_to_all(copies, axis, split_axis=0, concat_axis=0, tiled=True)


def over_copies(value, axis):
    everything = copy_for_each(value, axis)
    return jnp.sum(everything, axis=0)


def packed_total(arrays, axis):
    ravelled, at, finished = (jnp.concatenate([a.reshape(-1) for a in arrays]), 0, [])
    subtotal = over_copies(ravelled, axis)
    for a in arrays:
        finished.append(subtotal[at : at + a.size].reshape(a.shape))
        at += a.size
    return tuple(finished)


def rotate(values, positions):
    inverse = 1.0 / 10000.0 ** (jnp.arange(0, QK, 2, dtype=jnp.float32) / QK)
    angles = positions[:, None] * inverse[None, :]
    angles = jnp.concatenate([angles, angles], axis=-1)
    cosine = jnp.cos(angles)[:, None, None, :]
    sine = jnp.sin(angles)[:, None, None, :]
    first_half, second_half = jnp.split(values, 2, axis=-1)
    return values * cosine + jnp.concatenate([-second_half, first_half], axis=-1) * sine


def per_device(
    hidden_states,
    w_conv_b,
    w_conv_c,
    w_conv_h,
    conv_taps,
    w_query,
    w_key,
    w_value,
    lambdas,
    head_gain,
    w_out_conv,
    w_out_attn,
    out_gain,
):
    tok_rows = hidden_states.shape[0]
    head_count = w_value.shape[1] // VD
    channels = w_conv_b.shape[1]
    offset = lax.axis_index("sp") * tok_rows
    query_pos = offset + jnp.arange(tok_rows, dtype=jnp.int32)
    positions = query_pos.astype(jnp.float32)

    def project(weight):
        return jnp.dot(hidden_states, weight, preferred_element_type=jnp.float32).astype(
            jnp.bfloat16
        )

    key_rot = rotate(
        project(w_key).reshape(tok_rows, head_count, 2, QK).astype(jnp.float32), positions
    ).astype(jnp.bfloat16)
    values = project(w_value)
    query_rot = rotate(
        project(w_query).reshape(tok_rows, head_count, 2, QK).astype(jnp.float32), positions
    ).astype(jnp.bfloat16)
    scale = QK ** (-0.5)

    def attend(state, keys_blk, vals_blk, first_pos):
        running_max, running_sum, numer = state
        scores = (
            jnp.einsum("qhcd,khcd->hcqk", query_rot, keys_blk, preferred_element_type=jnp.float32)
            * scale
        )
        key_pos = first_pos + jnp.arange(keys_blk.shape[0], dtype=jnp.int32)
        visible = (key_pos[None, :] <= query_pos[:, None])[None, None]
        scores = jnp.where(visible, scores, NEG_LARGE)
        new_max = jnp.maximum(running_max, jnp.max(scores, axis=-1))
        weights = jnp.where(visible, jnp.exp(scores - new_max[..., None]), 0.0)
        factor = jnp.exp(running_max - new_max)
        running_sum = running_sum * factor + jnp.sum(weights, axis=-1)
        numer = numer * factor[..., None] + jnp.einsum(
            "hcqk,khe->hcqe",
            weights.astype(jnp.bfloat16),
            vals_blk,
            preferred_element_type=jnp.float32,
        )
        return (new_max, running_sum, numer)

    initial = (
        jnp.full((head_count, 2, tok_rows), NEG_LARGE, jnp.float32),
        jnp.zeros((head_count, 2, tok_rows), jnp.float32),
        jnp.zeros((head_count, 2, tok_rows, VD), jnp.float32),
    )
    packed_keys = key_rot.reshape(tok_rows, head_count * 2 * QK)
    key_piece, value_piece = sent_together((packed_keys, values), "sp", 0, 1)
    count = key_piece.shape[0]
    block = 512

    def one_block(index, state):
        first = index * block
        keys_blk = lax.dynamic_slice_in_dim(key_piece, first, block, 0).reshape(
            block, head_count, 2, QK
        )
        vals_blk = lax.dynamic_slice_in_dim(value_piece, first, block, 0).reshape(
            block, head_count, VD
        )
        return attend(state, keys_blk, vals_blk, first)

    def work(state):
        return lax.fori_loop(0, count // block, one_block, state)

    running_max, running_sum, numer = lax.cond(
        jnp.int32(0) <= offset + tok_rows - 1, work, lambda state: state, initial
    )
    u_b = project(w_conv_b)
    u_c = project(w_conv_c)
    u_h = project(w_conv_h)
    gated = u_c.astype(jnp.float32) * u_h.astype(jnp.float32)
    rim_rows = passed_along(gated[tok_rows - (TAPS - 1) :], "sp", 1)
    padded = jnp.concatenate([rim_rows, gated], axis=0)
    taps_f = conv_taps.astype(jnp.float32)
    convolved = jnp.zeros((tok_rows, channels), jnp.float32)
    for tap in range(TAPS):
        convolved = convolved + taps_f[tap][None, :] * padded[tap : tap + tok_rows]
    conv_out = (u_b.astype(jnp.float32) * convolved).astype(jnp.bfloat16)
    diff = (
        numer[:, 0] / running_sum[:, 0, :, None]
        - lambdas[:, None, None] * numer[:, 1] / running_sum[:, 1, :, None]
    )
    normed = (
        diff
        * lax.rsqrt(jnp.mean(diff * diff, axis=-1, keepdims=True) + 1e-05)
        * head_gain.astype(jnp.float32)[None, None, :]
    )
    attn_out = normed.astype(jnp.bfloat16).transpose(1, 0, 2).reshape(tok_rows, head_count * VD)
    gain_f = out_gain.astype(jnp.float32)
    partial_value = jnp.dot(conv_out, w_out_conv, preferred_element_type=jnp.float32) + jnp.dot(
        attn_out, w_out_attn, preferred_element_type=jnp.float32
    )
    summed = lax.psum_scatter(
        partial_value.astype(jnp.bfloat16), "tp", scatter_dimension=1, tiled=True
    )
    mix_f = summed.astype(jnp.float32)
    width = mix_f.shape[1]
    total_sum, total_squares = packed_total(
        (jnp.sum(mix_f, axis=-1), jnp.sum(mix_f * mix_f, axis=-1)), "tp"
    )
    mean_value = (total_sum / D)[:, None]
    variance = (total_squares / D)[:, None] - mean_value * mean_value
    own_gain = lax.dynamic_slice_in_dim(gain_f, lax.axis_index("tp") * width, width, 0)
    return ((mix_f - mean_value) * lax.rsqrt(variance + 1e-05) * own_gain[None, :]).astype(
        jnp.bfloat16
    )


def solution(mesh):
    return jax.shard_map(
        per_device,
        mesh=mesh,
        in_specs=(
            P("sp", None),
            P(None, "tp"),
            P(None, "tp"),
            P(None, "tp"),
            P(None, "tp"),
            P(None, "tp"),
            P(None, "tp"),
            P(None, "tp"),
            P("tp"),
            P(),
            P("tp", None),
            P("tp", None),
            P(),
        ),
        out_specs=P("sp", "tp"),
        check_vma=False,
    )
```

profile of v0, /device:TPU:1, one launch (start us, length us, event | category | flops | bytes accessed | tf_op | source)
XLA Modules:
  0.0 577.5 jit_solution(4355344827414637134)
XLA Ops:
  6.6 5.4 convolution_convert_fusion
  19.0 4.7 convolution_convert_fusion.1
  24.7 5.3 fusion.21
  30.1 4.6 fusion.20
  39.4 14.7 %fusion.37 = f32[768,4096]{1,0:T(8,128)} fusion(bf16[256,4096]{1,0:T(8,128)(2,1)S(1)} %copy-done, f32[2,256]{1,0:T(2,128)S(1)} %collective-permute-done, f32[768,256]{1,0:T(8,128)S(1)} %fusion.20, bf16[768,4096]{1,0:T(8,128)(2,1)} %param.17, bf16[4096,256]{1,0:T(8,128)(2,1)} %param.18, f32[256]{0:T(256)S(1)} %bitcast.103, f32[256]{0:T(256)S(1)} %bitcast.102, ...), kind=kOutput, calls=%fused_computation.67 | convolution fusion | flops 3223388160 | bytes 23860224 | tf_op jit(solution)/shard_map/dot_general | solution.py:164
  54.0 63.9 %all-gather.2.cloned.1.call-done = bf16[12288,512]{0,1:T(8,128)(2,1)} async-done(((bf16[768,512]{0,1:T(8,128)(2,1)}), bf16[12288,512]{0,1:T(8,128)(2,1)}) %all-gather.2.cloned.1.call-update) | async-done | bytes 12582928 | tf_op jit(solution)/shard_map/all_gather | solution.py:17
  117.9 383.7 %conditional.1 = (f32[2,2,768]{2,1,0:T(2,128)}, f32[2,2,768,128]{3,2,1,0:T(8,128)}) conditional(s32[]{:T(128)} %convert_element_type.98, () %tuple.27, (bf16[12288,512]{0,1:T(8,128)(2,1)}, s32[]{:T(128)}, s32[768]{0:T(1024)S(1)}, bf16[768,2,2,64]{0,3,2,1:T(8,128)(2,1)S(1)}) %tuple.71), branch_computations={%region_0.0_spmd, %region_1.6_spmd} | conditional | flops 626016512 | bytes 76100944 | solution.py:139
  117.9 10.6 %fusion.49 = (bf16[12288,256]{0,1:T(8,128)(2,1)}, bf16[12288,256]{0,1:T(8,128)(2,1)}) fusion(bf16[12288,512]{0,1:T(8,128)(2,1)} %get-tuple-element.158), kind=kLoop, calls=%fused_computation.90 | loop fusion | bytes 25165824 | tf_op jit(solution)/shard_map/slice | solution.py:19
  128.5 373.1 %while.17 = (s32[]{:T(128)}, f32[2,2,768]{2,1,0:T(2,128)S(1)}, f32[2,2,768]{2,1,0:T(2,128)}, f32[2,2,768,128]{3,2,1,0:T(8,128)}, s32[768]{0:T(1024)S(1)}, /*inde...) while((s32[]{:T(128)}, f32[2,2,768]{2,1,0:T(2,128)S(1)}, ...), condition=%wide.region_5.5_spmd.clone, body=%wide.region_2.4_spmd.clone.sunk | while | flops 626015744 | bytes 50928848 | solution.py:137
  153.4 4.5 fusion.87
  169.0 4.5 fusion.87
  184.6 4.5 fusion.87
  200.3 4.5 fusion.87
  215.9 4.5 fusion.87
  231.5 4.5 fusion.87
  247.1 4.5 fusion.87
  262.7 4.5 fusion.87
  278.4 4.5 fusion.87
  294.0 4.5 fusion.87
  309.6 4.5 fusion.87
  325.2 4.5 fusion.87
  340.8 4.5 fusion.87
  356.5 4.5 fusion.87
  372.1 4.5 fusion.87
  387.7 4.5 fusion.87
  403.3 4.5 fusion.87
  419.0 4.5 fusion.87
  434.6 4.5 fusion.87
  450.2 4.5 fusion.87
  481.4 4.5 fusion.87
  505.9 9.1 %add_convert_fusion = bf16[768,4096]{1,0:T(8,128)(2,1)} fusion(f32[768,4096]{1,0:T(8,128)} %fusion.37, bf16[768,256]{0,1:T(8,128)(2,1)S(1)} %bitcast.98, bf16[256,4096]{1,0:T(8,128)(2,1)S(1)} %copy-done.4), kind=kOutput, calls=%fused_computation.22 | convolution fusion | flops 1616904192 | bytes 21364736 | tf_op jit(solution)/shard_map/dot_general | solution.py:164
  515.0 41.8 %reduce-scatter.2.cloned.1.call-done = bf16[768,512]{1,0:T(8,128)(2,1)} async-done(((bf16[768,4096]{1,0:T(8,128)(2,1)}), bf16[768,512]{1,0:T(8,128)(2,1)}) %reduce-scatter.2.cloned.1.call-update) | async-done | bytes 786448 | tf_op jit(solution)/shard_map/reduce_scatter | solution.py:167
  (308 shorter events, 307.8 us)
Async XLA Ops:
  6.5 32.8 %copy-start = (bf16[256,4096]{1,0:T(8,128)(2,1)S(1)}, bf16[256,4096]{1,0:T(8,128)(2,1)}, u32[]{:S(2)}) copy-start(bf16[256,4096]{1,0:T(8,128)(2,1)} %param.27) | copy-start | bytes 6291460
  6.5 111.4 %all-gather.2.cloned.1.call-start = ((), (), s32[]{:S(2)}) async-start(), calls=%async_computation.2 | async-start | bytes 13369344 | tf_op jit(solution)/shard_map/all_gather | solution.py:17
  6.6 7.1 %copy-start.3 = (bf16[768,4096]{1,0:T(8,128)(2,1)S(1)}, bf16[768,4096]{1,0:T(8,128)(2,1)}, u32[]{:S(2)}) copy-start(bf16[768,4096]{1,0:T(8,128)(2,1)} %param.17) | copy-start | bytes 18874372
  6.6 7.1 %copy-start.9 = (bf16[4096,256]{1,0:T(8,128)(2,1)S(1)}, bf16[4096,256]{1,0:T(8,128)(2,1)}, u32[]{:S(2)}) copy-start(bf16[4096,256]{1,0:T(8,128)(2,1)} %param.23) | copy-start | bytes 6291460
  24.6 532.2 %reduce-scatter.2.cloned.1.call-start = ((), (), s32[]{:S(2)}) async-start(), calls=%async_computation.3 | async-start | bytes 7077888 | tf_op jit(solution)/shard_map/reduce_scatter | solution.py:167
  30.1 8.8 %copy-start.7 = (bf16[3,256]{1,0:T(4,128)(2,1)S(1)}, bf16[3,256]{1,0:T(4,128)(2,1)}, u32[]{:S(2)}) copy-start(bf16[3,256]{1,0:T(4,128)(2,1)} %param.21) | copy-start | bytes 4612
  30.1 8.8 %copy-start.12 = (bf16[128]{0:T(256)(128)(2,1)S(1)}, bf16[128]{0:T(256)(128)(2,1)}, u32[]{:S(2)}) copy-start(bf16[128]{0:T(256)(128)(2,1)} %param.26) | copy-start | bytes 772
  34.7 4.7 collective-permute-start
  39.4 78.5 %copy-start.6 = (bf16[768,2,2,64]{0,3,2,1:T(8,128)(2,1)S(1)}, bf16[768,2,2,64]{0,3,2,1:T(8,128)(2,1)}, u32[]{:S(2)}) copy-start(bf16[768,2,2,64]{0,3,2,1:T(8,128)(2,1)} %get-tuple-element.227) | copy-start | bytes 1179652
  147.5 5.8 %copy-start.2 = (f32[2,2,512,768]{3,2,1,0:T(8,128)S(1)}, f32[2,2,512,768]{3,2,1,0:T(8,128)}, u32[]{:S(2)}) copy-start(f32[2,2,512,768]{3,2,1,0:T(8,128)} %get-tuple-element.296) | copy-start | bytes 18874372 | tf_op jit(solution)/shard_map/cond/branch_1_fun/while
  163.2 5.8 %copy-start.2 = (f32[2,2,512,768]{3,2,1,0:T(8,128)S(1)}, f32[2,2,512,768]{3,2,1,0:T(8,128)}, u32[]{:S(2)}) copy-start(f32[2,2,512,768]{3,2,1,0:T(8,128)} %get-tuple-element.296) | copy-start | bytes 18874372 | tf_op jit(solution)/shard_map/cond/branch_1_fun/while
  178.8 5.8 %copy-start.2 = (f32[2,2,512,768]{3,2,1,0:T(8,128)S(1)}, f32[2,2,512,768]{3,2,1,0:T(8,128)}, u32[]{:S(2)}) copy-start(f32[2,2,512,768]{3,2,1,0:T(8,128)} %get-tuple-element.296) | copy-start | bytes 18874372 | tf_op jit(solution)/shard_map/cond/branch_1_fun/while
  194.4 5.8 %copy-start.2 = (f32[2,2,512,768]{3,2,1,0:T(8,128)S(1)}, f32[2,2,512,768]{3,2,1,0:T(8,128)}, u32[]{:S(2)}) copy-start(f32[2,2,512,768]{3,2,1,0:T(8,128)} %get-tuple-element.296) | copy-start | bytes 18874372 | tf_op jit(solution)/shard_map/cond/branch_1_fun/while
  210.0 5.8 %copy-start.2 = (f32[2,2,512,768]{3,2,1,0:T(8,128)S(1)}, f32[2,2,512,768]{3,2,1,0:T(8,128)}, u32[]{:S(2)}) copy-start(f32[2,2,512,768]{3,2,1,0:T(8,128)} %get-tuple-element.296) | copy-start | bytes 18874372 | tf_op jit(solution)/shard_map/cond/branch_1_fun/while
  225.7 5.8 %copy-start.2 = (f32[2,2,512,768]{3,2,1,0:T(8,128)S(1)}, f32[2,2,512,768]{3,2,1,0:T(8,128)}, u32[]{:S(2)}) copy-start(f32[2,2,512,768]{3,2,1,0:T(8,128)} %get-tuple-element.296) | copy-start | bytes 18874372 | tf_op jit(solution)/shard_map/cond/branch_1_fun/while
  241.3 5.8 %copy-start.2 = (f32[2,2,512,768]{3,2,1,0:T(8,128)S(1)}, f32[2,2,512,768]{3,2,1,0:T(8,128)}, u32[]{:S(2)}) copy-start(f32[2,2,512,768]{3,2,1,0:T(8,128)} %get-tuple-element.296) | copy-start | bytes 18874372 | tf_op jit(solution)/shard_map/cond/branch_1_fun/while
  256.9 5.8 %copy-start.2 = (f32[2,2,512,768]{3,2,1,0:T(8,128)S(1)}, f32[2,2,512,768]{3,2,1,0:T(8,128)}, u32[]{:S(2)}) copy-start(f32[2,2,512,768]{3,2,1,0:T(8,128)} %get-tuple-element.296) | copy-start | bytes 18874372 | tf_op jit(solution)/shard_map/cond/branch_1_fun/while
  272.5 5.8 %copy-start.2 = (f32[2,2,512,768]{3,2,1,0:T(8,128)S(1)}, f32[2,2,512,768]{3,2,1,0:T(8,128)}, u32[]{:S(2)}) copy-start(f32[2,2,512,768]{3,2,1,0:T(8,128)} %get-tuple-element.296) | copy-start | bytes 18874372 | tf_op jit(solution)/shard_map/cond/branch_1_fun/while
  288.1 5.8 %copy-start.2 = (f32[2,2,512,768]{3,2,1,0:T(8,128)S(1)}, f32[2,2,512,768]{3,2,1,0:T(8,128)}, u32[]{:S(2)}) copy-start(f32[2,2,512,768]{3,2,1,0:T(8,128)} %get-tuple-element.296) | copy-start | bytes 18874372 | tf_op jit(solution)/shard_map/cond/branch_1_fun/while
  303.8 5.8 %copy-start.2 = (f32[2,2,512,768]{3,2,1,0:T(8,128)S(1)}, f32[2,2,512,768]{3,2,1,0:T(8,128)}, u32[]{:S(2)}) copy-start(f32[2,2,512,768]{3,2,1,0:T(8,128)} %get-tuple-element.296) | copy-start | bytes 18874372 | tf_op jit(solution)/shard_map/cond/branch_1_fun/while
  319.4 5.8 %copy-start.2 = (f32[2,2,512,768]{3,2,1,0:T(8,128)S(1)}, f32[2,2,512,768]{3,2,1,0:T(8,128)}, u32[]{:S(2)}) copy-start(f32[2,2,512,768]{3,2,1,0:T(8,128)} %get-tuple-element.296) | copy-start | bytes 18874372 | tf_op jit(solution)/shard_map/cond/branch_1_fun/while
  335.0 5.8 %copy-start.2 = (f32[2,2,512,768]{3,2,1,0:T(8,128)S(1)}, f32[2,2,512,768]{3,2,1,0:T(8,128)}, u32[]{:S(2)}) copy-start(f32[2,2,512,768]{3,2,1,0:T(8,128)} %get-tuple-element.296) | copy-start | bytes 18874372 | tf_op jit(solution)/shard_map/cond/branch_1_fun/while
  350.6 5.8 %copy-start.2 = (f32[2,2,512,768]{3,2,1,0:T(8,128)S(1)}, f32[2,2,512,768]{3,2,1,0:T(8,128)}, u32[]{:S(2)}) copy-start(f32[2,2,512,768]{3,2,1,0:T(8,128)} %get-tuple-element.296) | copy-start | bytes 18874372 | tf_op jit(solution)/shard_map/cond/branch_1_fun/while
  366.2 5.8 %copy-start.2 = (f32[2,2,512,768]{3,2,1,0:T(8,128)S(1)}, f32[2,2,512,768]{3,2,1,0:T(8,128)}, u32[]{:S(2)}) copy-start(f32[2,2,512,768]{3,2,1,0:T(8,128)} %get-tuple-element.296) | copy-start | bytes 18874372 | tf_op jit(solution)/shard_map/cond/branch_1_fun/while
  381.9 5.8 %copy-start.2 = (f32[2,2,512,768]{3,2,1,0:T(8,128)S(1)}, f32[2,2,512,768]{3,2,1,0:T(8,128)}, u32[]{:S(2)}) copy-start(f32[2,2,512,768]{3,2,1,0:T(8,128)} %get-tuple-element.296) | copy-start | bytes 18874372 | tf_op jit(solution)/shard_map/cond/branch_1_fun/while
  397.5 5.8 %copy-start.2 = (f32[2,2,512,768]{3,2,1,0:T(8,128)S(1)}, f32[2,2,512,768]{3,2,1,0:T(8,128)}, u32[]{:S(2)}) copy-start(f32[2,2,512,768]{3,2,1,0:T(8,128)} %get-tuple-element.296) | copy-start | bytes 18874372 | tf_op jit(solution)/shard_map/cond/branch_1_fun/while
  413.1 5.8 %copy-start.2 = (f32[2,2,512,768]{3,2,1,0:T(8,128)S(1)}, f32[2,2,512,768]{3,2,1,0:T(8,128)}, u32[]{:S(2)}) copy-start(f32[2,2,512,768]{3,2,1,0:T(8,128)} %get-tuple-element.296) | copy-start | bytes 18874372 | tf_op jit(solution)/shard_map/cond/branch_1_fun/while
  428.7 5.8 %copy-start.2 = (f32[2,2,512,768]{3,2,1,0:T(8,128)S(1)}, f32[2,2,512,768]{3,2,1,0:T(8,128)}, u32[]{:S(2)}) copy-start(f32[2,2,512,768]{3,2,1,0:T(8,128)} %get-tuple-element.296) | copy-start | bytes 18874372 | tf_op jit(solution)/shard_map/cond/branch_1_fun/while
  444.4 5.8 %copy-start.2 = (f32[2,2,512,768]{3,2,1,0:T(8,128)S(1)}, f32[2,2,512,768]{3,2,1,0:T(8,128)}, u32[]{:S(2)}) copy-start(f32[2,2,512,768]{3,2,1,0:T(8,128)} %get-tuple-element.296) | copy-start | bytes 18874372 | tf_op jit(solution)/shard_map/cond/branch_1_fun/while
  491.2 5.8 %copy-start.2 = (f32[2,2,512,768]{3,2,1,0:T(8,128)S(1)}, f32[2,2,512,768]{3,2,1,0:T(8,128)}, u32[]{:S(2)}) copy-start(f32[2,2,512,768]{3,2,1,0:T(8,128)} %get-tuple-element.296) | copy-start | bytes 18874372 | tf_op jit(solution)/shard_map/cond/branch_1_fun/while
  515.0 55.6 %copy-start.1 = (bf16[256,4096]{1,0:T(8,128)(2,1)S(1)}, bf16[256,4096]{1,0:T(8,128)(2,1)}, u32[]{:S(2)}) copy-start(bf16[256,4096]{1,0:T(8,128)(2,1)} %param.27) | copy-start | bytes 6291460
  558.9 9.3 %all-to-all-start = ((f32[8,1,1536]{2,1,0:T(1,128)}), f32[8,1,1536]{2,1,0:T(1,128)S(1)}, u32[]{:S(2)}, u32[]{:S(2)}) async-start(f32[8,1,1536]{2,1,0:T(1,128)} %broadcast_in_dim.83), calls=%async_computation.1 | async-start | bytes 98304 | tf_op jit(solution)/shard_map/all_to_all | solution.py:32
  (8 other events, 29.8 us)
Sparse Core Ops, SparseCore 0:
  24.8 93.1 all-gather.1
  515.1 41.6 reduce-scatter.1
where the time goes:
time: 580 us; the launch traced here: 577 us
  matrix products  246 us (42%)
  other arithmetic  156 us (27%)
  waiting for transfers between devices  110 us (19%)
  local copies, waits for them, and re-layouts  42.3 us (7%)
  between operations  13.7 us (2%)
  starting transfers between devices  8.63 us (1%)
    reduce_sum x24, other arithmetic, attend(): running_sum = running_sum * factor + jnp.sum(weights, axis=-1)  108 us
    dot_general x24, matrix products, attend(): jnp.einsum('hcqk,khe->hcqe', weights.astype(jnp.bfloat16), vals_blk, pref...  108 us
    dot_general x24, matrix products, attend(): jnp.einsum('qhcd,khcd->hcqk', query_rot, keys_blk, preferred_element_type...  92.5 us
    all_gather x1, waiting for transfers between devices, sent_together(): lax.all_gather(both, axis, axis=dim, tiled=True)  63.9 us
    reduce_scatter x1, waiting for transfers between devices, per_device(): lax.psum_scatter(partial_value.astype(jnp.bfloat16), 'tp', scatter_dimens...  41.8 us
    add x24, other arithmetic, attend(): running_sum = running_sum * factor + jnp.sum(weights, axis=-1)  31.5 us
    dynamic_slice x24, local copies, waits for them, and re-layouts, one_block(): lax.dynamic_slice_in_dim(value_piece, first, block, 0)  25.6 us
    dot_general x5, matrix products, project(): jnp.dot(hidden_states, weight, preferred_element_type=jnp.float32)  22 us
  transfers between devices with their start and end apart: 4, of which 4 were waited for; matrix products, arithmetic and copies ran while one was open for 4% of the time, Pallas kernels for 0%

commit v1 on v0

v1 whole, which is shorter than its diff:
```python
import functools

import jax
import jax.numpy as jnp
from jax import lax
from jax.experimental import pallas as pl
from jax.experimental.pallas import tpu as pltpu
from jax.sharding import PartitionSpec as P

D = 4096
QK = 64
TAPS = 3
VD = 128
TB = 768
NB = 16
TQ = 256
NT = TB // TQ
VA = 144
LOG2E = 1.4426950408889634
NEG_LARGE = -1e30
BF16 = jnp.bfloat16
F32 = jnp.float32


def attention_kernel(
    k_in, v_in, q_in, lam_in, gain_ref, o_hbm,
    k_all, v_all, q_own, qa, lam_own, s0, s1, s2, acc, m_ref, o_stage,
    k_recv, v_recv, q_recv, l_recv, o_recv,
    q_send, l_send, p1k_send, p1v_send, rk_send, rv_send, lk_send, lv_send,
    dk_send, dv_send, o_send,
):
    sp = lax.axis_index("sp")
    tp = lax.axis_index("tp")
    z, x = sp // 4, sp % 4
    y, c = tp // 2, tp % 2
    own_pair = 2 * x + c

    def device(zz, xx, cc):
        return {"sp": zz * 4 + xx, "tp": y * 2 + cc}

    def send(src, dst, send_sem, recv_sem, zz, xx, cc):
        same = (zz == z) & (xx == x) & (cc == c)

        @pl.when(same)
        def _():
            pltpu.make_async_copy(src, dst, recv_sem).start()

        @pl.when(jnp.logical_not(same))
        def _():
            remote(src, dst, send_sem, recv_sem, zz, xx, cc).start()

    def remote(src, dst, send_sem, recv_sem, zz, xx, cc):
        return pltpu.make_async_remote_copy(
            src_ref=src, dst_ref=dst, send_sem=send_sem, recv_sem=recv_sem,
            device_id=device(zz, xx, cc), device_id_type=pl.DeviceIdType.MESH,
        )

    def wait_sent(src, dst, send_sem, recv_sem, zz, xx, cc):
        same = (zz == z) & (xx == x) & (cc == c)

        @pl.when(jnp.logical_not(same))
        def _():
            remote(src, dst, send_sem, recv_sem, zz, xx, cc).wait_send()

    barrier = pltpu.get_barrier_semaphore()
    me = sp * 2 + c

    def greet(i, carry):
        other = (me + i) % 32
        pl.semaphore_signal(
            barrier, inc=1, device_id={"sp": other // 2, "tp": y * 2 + other % 2},
            device_id_type=pl.DeviceIdType.MESH,
        )
        return carry

    lax.fori_loop(1, 32, greet, 0)
    pl.semaphore_wait(barrier, 31)

    pair_of_sp = jnp.where(sp < 8, sp, 15 - sp)
    slot_of_sp = jnp.where(sp < 8, 0, 1)
    first = []
    for e in range(2):
        head = 2 * c + e
        first.append((k_in.at[:, e * 128 : (e + 1) * 128], k_all.at[sp], p1k_send.at[e], k_recv.at[sp], head, x, z % 2))
        first.append((q_in.at[e * 128 : (e + 1) * 128], q_own.at[slot_of_sp], q_send.at[e], q_recv.at[slot_of_sp], head, pair_of_sp // 2, pair_of_sp % 2))
        first.append((v_in.at[e * 128 : (e + 1) * 128], v_all.at[sp, pl.ds(0, 128)], p1v_send.at[e], v_recv.at[sp], head, x, z % 2))
        first.append((lam_in.at[e], lam_own.at[slot_of_sp], l_send.at[e], l_recv.at[slot_of_sp], head, pair_of_sp // 2, pair_of_sp % 2))
    for one in first:
        send(*one)

    def ones(j, carry):
        v_all[j, 128:VA, :] = jnp.ones((VA - 128, TB), BF16)
        return carry

    lax.fori_loop(0, NB, ones, 0)
    acc[...] = jnp.zeros(acc.shape, F32)
    m_ref[...] = jnp.full(m_ref.shape, NEG_LARGE, F32)
    zero = jnp.zeros((QK, TQ), BF16)
    for qb in range(2):
        remote(q_in.at[0:128], q_own.at[qb], q_send.at[0], q_recv.at[qb], z, x, c).wait_recv()
        remote(lam_in.at[0], lam_own.at[qb], l_send.at[0], l_recv.at[qb], z, x, c).wait_recv()
        for t in range(NT):
            qt = q_own[qb, :, t * TQ : (t + 1) * TQ]
            qa[qb * NT + t, 0:QK, 0:TQ] = qt[0:QK]
            qa[qb * NT + t, QK:128, 0:TQ] = zero
            qa[qb * NT + t, 0:QK, TQ : 2 * TQ] = zero
            qa[qb * NT + t, QK:128, TQ : 2 * TQ] = qt[QK:128]

    scores = (s0, s1, s2)

    def unit(qb, j, diagonal):
        tops = [None] * NT

        def produce(t):
            rows = TQ * (t + 1) if diagonal else TB
            s = jnp.dot(k_all[j, 0:rows, :], qa[qb * NT + t], preferred_element_type=F32)
            if diagonal:
                key = lax.broadcasted_iota(jnp.int32, (rows, 2 * TQ), 0)
                query = lax.broadcasted_iota(jnp.int32, (rows, 2 * TQ), 1)
                query = jnp.where(query >= TQ, query - TQ, query) + t * TQ
                s = jnp.where(key <= query, s, NEG_LARGE)
            scores[t][0:rows, :] = s
            tops[t] = jnp.max(s, axis=0, keepdims=True)

        def consume(t):
            rows = TQ * (t + 1) if diagonal else TB
            at = qb * NT + t
            before = m_ref[at]
            after = jnp.maximum(before, tops[t])
            w = jnp.exp2(scores[t][0:rows, :] - after).astype(BF16)
            factor = jnp.exp2(before - after)
            acc[at] = acc[at] * factor + jnp.dot(
                v_all[j, :, 0:rows], w, preferred_element_type=F32
            )
            m_ref[at] = after

        produce(0)
        produce(1)
        consume(0)
        produce(2)
        consume(1)
        consume(2)

    def block_of(i):
        w, u = i // 4, i % 4
        side = jnp.where(u < 2, x + 3, x + 1) % 4
        col = jnp.where(w == 0, x, jnp.where(w == 3, (x + 2) % 4, side))
        row = jnp.where(w == 2, (u + 2) % 4, u)
        return w, u, row * 4 + col

    left, right = (x + 3) % 4, (x + 1) % 4

    def k_copy(blk, sems, n, zz, xx, cc):
        return remote(k_all.at[blk], k_all.at[blk], sems.at[n], k_recv.at[blk], zz, xx, cc)

    def v_copy(blk, sems, n, zz, xx, cc):
        part = v_all.at[blk, pl.ds(0, 128)]
        return remote(part, part, sems.at[n], v_recv.at[blk], zz, xx, cc)

    def step(i, carry):
        w, u, blk = block_of(i)
        k_copy(blk, dk_send, 0, z, x, 1 - c).wait_recv()
        v_copy(blk, dv_send, 0, z, x, 1 - c).wait_recv()

        @pl.when(u % 2 == c)
        def _():
            @pl.when((w == 0) & (u < 2))
            def _():
                k_copy(blk, rk_send, 0, z, right, c).start()
                v_copy(blk, rv_send, 0, z, right, c).start()

            @pl.when((w == 0) & (u >= 2))
            def _():
                k_copy(blk, lk_send, 0, z, left, c).start()
                v_copy(blk, lv_send, 0, z, left, c).start()
                k_copy(blk, rk_send, 1, z, right, c).start()
                v_copy(blk, rv_send, 1, z, right, c).start()
                k_copy(blk - 8, lk_send, 1, z, left, c).start()
                v_copy(blk - 8, lv_send, 1, z, left, c).start()

            @pl.when((w == 1) & (u < 2))
            def _():
                k_copy(blk, rk_send, 2, z, right, c).start()
                v_copy(blk, rv_send, 2, z, right, c).start()

            @pl.when((w == 1) & (u >= 2))
            def _():
                k_copy(blk, lk_send, 2, z, left, c).start()
                v_copy(blk, lv_send, 2, z, left, c).start()

            k_copy(blk, dk_send, i // 2, z, x, 1 - c).start()
            v_copy(blk, dv_send, i // 2, z, x, 1 - c).start()

        def for_queries(qb, carry):
            q_blk = jnp.where(qb == 0, own_pair, 15 - own_pair)

            @pl.when(blk < q_blk)
            def _():
                unit(qb, blk, False)

            @pl.when(blk == q_blk)
            def _():
                unit(qb, blk, True)

            return carry

        lax.fori_loop(0, 2, for_queries, 0)
        return carry

    lax.fori_loop(0, NB, step, 0)

    out = []
    for qb in range(2):
        lam = lam_own[qb, 0:1, 0:1]
        for t in range(NT):
            at = qb * NT + t
            n1 = acc[at, 0:128, 0:TQ] / acc[at, 128:129, 0:TQ]
            n2 = acc[at, 0:128, TQ : 2 * TQ] / acc[at, 128:129, TQ : 2 * TQ]
            diff = n1 - lam * n2
            mean = jnp.mean(diff * diff, axis=0, keepdims=True)
            o_stage[qb, :, t * TQ : (t + 1) * TQ] = (
                diff * lax.rsqrt(mean + 1e-05) * gain_ref[...]
            ).astype(BF16)
        q_blk = own_pair if qb == 0 else 15 - own_pair
        e = z % 2
        one = (o_stage.at[qb], o_hbm.at[e], o_send.at[qb], o_recv.at[e], q_blk // 4, q_blk % 4, z // 2)
        send(*one)
        out.append(one)

    for one in first + out:
        wait_sent(*one)
    for n in range(3):
        k_copy(0, rk_send, n, z, right, c).wait_send()
        v_copy(0, rv_send, n, z, right, c).wait_send()
        k_copy(0, lk_send, n, z, left, c).wait_send()
        v_copy(0, lv_send, n, z, left, c).wait_send()
    for n in range(8):
        k_copy(0, dk_send, n, z, x, 1 - c).wait_send()
        v_copy(0, dv_send, n, z, x, 1 - c).wait_send()
    for e in range(2):
        remote(o_stage.at[e], o_hbm.at[e], o_send.at[e], o_recv.at[e], z, x, c).wait_recv()


def attention(keys, values_t, query_t, lam, gain):
    dma = pltpu.SemaphoreType.DMA
    hbm = pl.BlockSpec(memory_space=pl.ANY)
    return pl.pallas_call(
        attention_kernel,
        out_shape=jax.ShapeDtypeStruct((2, 128, TB), BF16),
        in_specs=[hbm, hbm, hbm, hbm, pl.BlockSpec(memory_space=pltpu.VMEM)],
        out_specs=hbm,
        scratch_shapes=[
            pltpu.VMEM((NB, TB, 128), BF16),
            pltpu.VMEM((NB, VA, TB), BF16),
            pltpu.VMEM((2, 128, TB), BF16),
            pltpu.VMEM((2 * NT, 128, 2 * TQ), BF16),
            pltpu.VMEM((2, 8, 128), F32),
            pltpu.VMEM((TB, 2 * TQ), F32),
            pltpu.VMEM((TB, 2 * TQ), F32),
            pltpu.VMEM((TB, 2 * TQ), F32),
            pltpu.VMEM((2 * NT, VA, 2 * TQ), F32),
            pltpu.VMEM((2 * NT, 1, 2 * TQ), F32),
            pltpu.VMEM((2, 128, TB), BF16),
            dma((NB,)), dma((NB,)), dma((2,)), dma((2,)), dma((2,)),
            dma((2,)), dma((2,)), dma((2,)), dma((2,)),
            dma((3,)), dma((3,)), dma((3,)), dma((3,)),
            dma((8,)), dma((8,)), dma((2,)),
        ],
        compiler_params=pltpu.CompilerParams(
            collective_id=0, has_side_effects=True, vmem_limit_bytes=48 << 20
        ),
        name="attention",
    )(keys, values_t, query_t, lam, gain)


def passed_along(block, axis, distance):
    devices = range(lax.axis_size(axis))
    route = [(i - distance, i) for i in devices if i - distance in devices]
    return lax.ppermute(block, axis, route)


def copy_for_each(value, axis):
    copies = jnp.broadcast_to(value, (lax.axis_size(axis), *value.shape))
    return lax.all_to_all(copies, axis, split_axis=0, concat_axis=0, tiled=True)


def per_device(
    hidden_states,
    w_conv_b,
    w_conv_c,
    w_conv_h,
    conv_taps,
    w_query,
    w_key,
    w_value,
    lambdas,
    head_gain,
    w_out_conv,
    w_out_attn,
    out_gain,
):
    tok_rows = hidden_states.shape[0]
    channels = w_conv_b.shape[1]
    offset = lax.axis_index("sp") * tok_rows
    positions = (offset + jnp.arange(tok_rows, dtype=jnp.int32)).astype(F32)
    inverse = 1.0 / 10000.0 ** (jnp.arange(0, QK, 2, dtype=F32) / QK)

    def project(weight):
        return jnp.dot(hidden_states, weight, preferred_element_type=F32).astype(BF16)

    def project_t(weight):
        return lax.dot_general(
            weight, hidden_states, (((0,), (1,)), ((), ())), preferred_element_type=F32
        ).astype(BF16)

    angles = positions[:, None] * inverse[None, :]
    cos, sin = jnp.cos(angles), jnp.sin(angles)

    k = project(w_key).astype(F32).reshape(tok_rows, 4, 2, QK // 2)
    k1, k2 = k[:, :, 0], k[:, :, 1]
    ck, sk = cos[:, None, :], sin[:, None, :]
    keys = jnp.stack([k1 * ck - k2 * sk, k2 * ck + k1 * sk], axis=2).reshape(tok_rows, 256).astype(BF16)

    scale = LOG2E * QK ** (-0.5)
    cq, sq = (cos.T * scale)[None], (sin.T * scale)[None]
    q = project_t(w_query).astype(F32).reshape(4, 2, QK // 2, tok_rows)
    q1, q2 = q[:, 0], q[:, 1]
    query_t = jnp.stack([q1 * cq - q2 * sq, q2 * cq + q1 * sq], axis=1).reshape(256, tok_rows).astype(BF16)
    values_t = project_t(w_value)

    lam = jnp.broadcast_to(lambdas[:, None, None], (2, 8, 128))
    gain = head_gain.astype(F32)[:, None]
    attn_t = attention(keys, values_t, query_t, lam, gain).reshape(256, tok_rows)

    u_b = project(w_conv_b)
    u_c = project(w_conv_c)
    u_h = project(w_conv_h)
    gated = u_c.astype(F32) * u_h.astype(F32)
    rim_rows = passed_along(gated[tok_rows - (TAPS - 1) :], "sp", 1)
    padded = jnp.concatenate([rim_rows, gated], axis=0)
    taps_f = conv_taps.astype(F32)
    convolved = jnp.zeros((tok_rows, channels), F32)
    for tap in range(TAPS):
        convolved = convolved + taps_f[tap][None, :] * padded[tap : tap + tok_rows]
    conv_out = (u_b.astype(F32) * convolved).astype(BF16)

    gain_f = out_gain.astype(F32)
    partial_value = jnp.dot(conv_out, w_out_conv, preferred_element_type=F32) + lax.dot_general(
        attn_t, w_out_attn, (((0,), (0,)), ((), ())), preferred_element_type=F32
    )
    summed = lax.psum_scatter(partial_value.astype(BF16), "tp", scatter_dimension=1, tiled=True)
    mix_f = summed.astype(F32)
    width = mix_f.shape[1]
    stats = jnp.concatenate([jnp.sum(mix_f, axis=-1), jnp.sum(mix_f * mix_f, axis=-1)])
    total = jnp.sum(copy_for_each(stats, "tp").reshape(lax.axis_size("tp"), -1), axis=0)
    mean_value = (total[:tok_rows] / D)[:, None]
    variance = (total[tok_rows:] / D)[:, None] - mean_value * mean_value
    own_gain = lax.dynamic_slice_in_dim(gain_f, lax.axis_index("tp") * width, width, 0)
    return ((mix_f - mean_value) * lax.rsqrt(variance + 1e-05) * own_gain[None, :]).astype(BF16)


def solution(mesh):
    return jax.shard_map(
        per_device,
        mesh=mesh,
        in_specs=(
            P("sp", None),
            P(None, "tp"),
            P(None, "tp"),
            P(None, "tp"),
            P(None, "tp"),
            P(None, "tp"),
            P(None, "tp"),
            P(None, "tp"),
            P("tp"),
            P(),
            P("tp", None),
            P("tp", None),
            P(),
        ),
        out_specs=P("sp", "tp"),
        check_vma=False,
    )
```

time: 580 us -> 204 us (0.35)
  matrix products: 246 us -> 42.1 us
  other arithmetic: 156 us -> 5.86 us
  Pallas kernels: 0 us -> 84.5 us
  waiting for transfers between devices: 110 us -> 45 us
  local copies, waits for them, and re-layouts: 42.3 us -> 3.68 us
    dot_general x55 -> x7, matrix products: 246 us -> 42.1 us  [the longest x1 15.3 us: per_device(): jnp.dot(conv_out, w_out_conv, preferred_element_type=F32)]
    reduce_sum x26 -> x1, other arithmetic: 108 us -> 0.04 us  [per_device(): jnp.sum(copy_for_each(stats, 'tp').reshape(lax.axis_size('tp'), -1), axis=0)]
    pallas_call x0 -> x1, Pallas kernels: none -> 84.5 us  [attention(): pl.pallas_call(attention_kernel, out_shape=jax.ShapeDtypeStruct((2, 128,...]
    all_gather x1 -> x0, waiting for transfers between devices: 63.9 us -> none  [sent_together(): lax.all_gather(both, axis, axis=dim, tiled=True)]
    add x49 -> x0, other arithmetic: 31.6 us -> none  [the longest x24 31.5 us: attend(): running_sum = running_sum * factor + jnp.sum(weights, axis=-1)]
    dynamic_slice x24 -> x0, local copies, waits for them, and re-layouts: 25.6 us -> none  [one_block(): lax.dynamic_slice_in_dim(value_piece, first, block, 0)]
    slice x2 -> x0, local copies, waits for them, and re-layouts: 11.3 us -> none  [the longest x1 10.6 us: sent_together(): lax.slice_in_dim(filled, at, at + a.shape[along], axis=along)]
    le x24 -> x0, other arithmetic: 6.87 us -> none  [attend(): visible = (key_pos[None, :] <= query_pos[:, None])[None, None]]
  transfers between devices with their start and end apart: 4 -> 3, of which waited for: 4 -> 2; matrix products, arithmetic and copies ran while one was open for 4% -> 6% of each run, Pallas kernels for 0% -> 42%
where the time goes in v1:
time: 204 us; the launch traced here: 203 us
  Pallas kernels  84.5 us (41%)
  waiting for transfers between devices  45 us (22%)
  matrix products  42.1 us (21%)
  between operations  13.7 us (7%)
  starting transfers between devices  8.41 us (4%)
  other arithmetic  5.86 us (3%)
  local copies, waits for them, and re-layouts  3.68 us (2%)
    pallas_call x1, Pallas kernels, attention(): pl.pallas_call(attention_kernel, out_shape=jax.ShapeDtypeStruct((2, 128,...  84.5 us
    reduce_scatter x1, waiting for transfers between devices, per_device(): lax.psum_scatter(partial_value.astype(BF16), 'tp', scatter_dimension=1, t...  40.9 us
    dot_general x1, matrix products, per_device(): jnp.dot(conv_out, w_out_conv, preferred_element_type=F32)  15.3 us
    dot_general x3, matrix products, project(): jnp.dot(hidden_states, weight, preferred_element_type=F32).astype(BF16)  12.8 us
    dot_general x1, matrix products, per_device(): lax.dot_general(attn_t, w_out_attn, (((0,), (0,)), ((), ())), preferred_e...  9.64 us
    all_to_all x1, starting transfers between devices, copy_for_each(): return lax.all_to_all(copies, axis, split_axis=0, concat_axis=0, tiled=True)  4.49 us
    dot_general x2, matrix products, project_t(): lax.dot_general(weight, hidden_states, (((0,), (1,)), ((), ())), preferre...  4.44 us
  transfers between devices with their start and end apart: 3, of which 2 were waited for; matrix products, arithmetic and copies ran while one was open for 6% of the time, Pallas kernels for 42%

profile of v1, /device:TPU:1, one launch (start us, length us, event | category | flops | bytes accessed | tf_op | source)
XLA Modules:
  0.0 203.2 jit_solution(4200467364123029407)
XLA Ops:
  6.5 5.4 %fusion.6 = f32[768,256]{1,0:T(8,128)S(1)} fusion(bf16[768,4096]{1,0:T(8,128)(2,1)} %param.13, bf16[4096,256]{1,0:T(8,128)(2,1)} %param.15), kind=kOutput, calls=%fused_computation.15 | convolution fusion | flops 1611005952 | bytes 9175040 | tf_op jit(solution)/shard_map/dot_general | solution.py:309
  11.9 0.6 copy-done.6
  12.5 1.8 fusion.5
  14.3 0.9 copy-done.3
  15.2 3.9 %collective-permute-start = (f32[2,256]{1,0:T(2,128)S(1)}, f32[2,256]{1,0:T(2,128)S(1)}, u32[]{:S(2)}, u32[]{:S(2)}) collective-permute-start(f32[2,256]{1,0:T(2,128)S(1)} %slice.49), channel_id=1, source_target_pairs={{0,8},{8,16},{16,24},{24,32},{32,40},{40,48},{48,56},{56,64},{64,7... | collective-permute-start | bytes 6152 | tf_op jit(solution)/shard_map/ppermute | solution.py:279
  19.2 0.0 slice-start
  19.2 0.4 multiply_cosine_fusion.1
  19.6 0.4 fusion.20
  20.0 0.0 slice-start.1
  20.1 5.6 %convolution_convert_fusion.2 = bf16[768,256]{0,1:T(8,128)(2,1)S(1)} fusion(bf16[768,4096]{1,0:T(8,128)(2,1)} %param.13, bf16[4096,256]{1,0:T(8,128)(2,1)} %param.19), kind=kOutput, calls=%fused_computation.10 | convolution fusion | flops 1610809344 | bytes 8781824 | tf_op jit(solution)/shard_map/dot_general | solution.py:309
  25.7 0.1 convert.19
  25.8 1.8 convolution_convert_fusion
  27.6 0.1 convert.20
  27.7 2.6 %convolution_convert_fusion.1.v_in = bf16[256,768]{1,0:T(8,128)(2,1)} fusion(bf16[4096,256]{1,0:T(8,128)(2,1)S(1)} %copy-done.8, bf16[768,4096]{1,0:T(8,128)(2,1)S(1)} %bitcast.31), kind=kOutput, calls=%fused_computation.9 | convolution fusion | flops 1610809344 | bytes 8781824 | tf_op jit(solution)/shard_map/dot_general | solution.py:312
  30.4 0.1 subtract_convert_fusion.1
  30.5 0.1 subtract_convert_fusion
  30.7 0.2 copy.21.k_in
  30.8 0.1 copy.22.gain_ref
  31.0 0.2 copy-done.5
  31.1 0.1 broadcast_in_dim.8.lam_in
  31.2 1.0 copy-done.1
  32.2 84.5 %attention.1 = bf16[2,128,768]{2,1,0:T(8,128)(2,1)S(1)} custom-call(bf16[768,256]{1,0:T(8,128)(2,1)S(1)} %copy.21.k_in, bf16[256,768]{1,0:T(8,128)(2,1)S(1)} %copy-done.1, bf16[256,768]{1,0:T(8,128)(2,1)S(1)} %bitcast.29, f32[2,8,128]{2,1,0:T(8,128)S(1)} %broadcast_in_dim.8.lam_in, f32[128,1]{1,0:T(8,128)S(1)} %copy.22.gain_ref), custom_call_target="tpu_custom_call" | custom-call | tf_op jit(solution)/shard_map/attention/pallas_call | solution.py:247
  116.7 15.3 %fusion.15 = f32[768,4096]{1,0:T(8,128)} fusion(bf16[256,4096]{1,0:T(8,128)(2,1)S(1)} %copy-done, f32[2,256]{1,0:T(2,128)S(1)} %collective-permute-done, f32[768,256]{1,0:T(8,128)} %copy-done.3, bf16[768,4096]{1,0:T(8,128)(2,1)} %param.13, bf16[4096,256]{1,0:T(8,128)(2,1)} %param.14, f32[256]{0:T(256)S(1)} %bitcast.37, f32[256]{0:T(256)S(1)} %bitcast.36, ...), kind=kOutput, calls=%fused_computation.28 | convolution fusion | flops 3223388160 | bytes 23860224 | tf_op jit(solution)/shard_map/dot_general | solution.py:348
  132.0 9.6 %add_convert_fusion = bf16[768,4096]{1,0:T(8,128)(2,1)} fusion(f32[768,4096]{1,0:T(8,128)} %fusion.15, bf16[256,768]{1,0:T(8,128)(2,1)S(1)} %bitcast.28, bf16[256,4096]{1,0:T(8,128)(2,1)} %param.24), kind=kOutput, calls=%fused_computation | convolution fusion | flops 1616904192 | bytes 21364736 | tf_op jit(solution)/shard_map/dot_general | solution.py:348
  141.6 0.0 reduce-scatter.2.cloned.1.call-update
  141.6 40.9 %reduce-scatter.2.cloned.1.call-done = bf16[768,512]{1,0:T(8,128)(2,1)} async-done(((bf16[768,4096]{1,0:T(8,128)(2,1)}), bf16[768,512]{1,0:T(8,128)(2,1)}) %reduce-scatter.2.cloned.1.call-update) | async-done | bytes 786448 | tf_op jit(solution)/shard_map/reduce_scatter | solution.py:351
  182.6 1.4 convert_reduce_fusion
  184.0 0.7 broadcast_in_dim.11
  184.6 4.5 %all-to-all-start = ((f32[8,1,1536]{2,1,0:T(1,128)}), f32[8,1,1536]{2,1,0:T(1,128)S(1)}, u32[]{:S(2)}, u32[]{:S(2)}) async-start(f32[8,1,1536]{2,1,0:T(1,128)} %broadcast_in_dim.11), calls=%async_computation.1 | async-start | bytes 98304 | tf_op jit(solution)/shard_map/all_to_all | solution.py:284
  189.1 0.8 dynamic-slice_convert_fusion
  189.9 4.0 %all-to-all-done = f32[8,1,1536]{2,1,0:T(1,128)S(1)} async-done(((f32[8,1,1536]{2,1,0:T(1,128)}), f32[8,1,1536]{2,1,0:T(1,128)S(1)}, u32[]{:S(2)}, u32[]{:S(2)}) %all-to-all-start) | async-done | bytes 49184 | tf_op jit(solution)/shard_map/all_to_all | solution.py:284
  194.0 2.4 %fusion.3 = bf16[768,512]{1,0:T(8,128)(2,1)} fusion(bf16[768,512]{1,0:T(8,128)(2,1)} %reduce-scatter.2.cloned.1.call-done, f32[512]{0:T(512)S(1)} %dynamic-slice_convert_fusion, f32[768]{0:T(1024)S(1)} %get-tuple-element.12, f32[768]{0:T(1024)S(1)} %get-tuple-element.11), kind=kLoop, calls=%fused_computation.7 | loop fusion | flops 1966080 | bytes 1581056 | tf_op jit(solution)/shard_map/convert_element_type | solution.py:359
  (31 shorter events, 0.2 us)
Async XLA Ops:
  6.5 110.2 %copy-start = (bf16[256,4096]{1,0:T(8,128)(2,1)S(1)}, bf16[256,4096]{1,0:T(8,128)(2,1)}, u32[]{:S(2)}) copy-start(bf16[256,4096]{1,0:T(8,128)(2,1)} %param.23) | copy-start | bytes 6291460
  6.5 176.0 %reduce-scatter.2.cloned.1.call-start = ((), (), s32[]{:S(2)}) async-start(), calls=%async_computation.2 | async-start | bytes 7077888 | tf_op jit(solution)/shard_map/reduce_scatter | solution.py:351
  6.5 5.4 %copy-start.2 = (bf16[768,4096]{1,0:T(8,128)(2,1)S(1)}, bf16[768,4096]{1,0:T(8,128)(2,1)}, u32[]{:S(2)}) copy-start(bf16[768,4096]{1,0:T(8,128)(2,1)} %param.13) | copy-start | bytes 18874372
  6.5 6.0 %copy-start.6 = (bf16[4096,256]{1,0:T(8,128)(2,1)S(1)}, bf16[4096,256]{1,0:T(8,128)(2,1)}, u32[]{:S(2)}) copy-start(bf16[4096,256]{1,0:T(8,128)(2,1)} %param.16) | copy-start | bytes 6291460
  14.3 0.9 copy-start.3
  15.2 101.5 %collective-permute-start = (f32[2,256]{1,0:T(2,128)S(1)}, f32[2,256]{1,0:T(2,128)S(1)}, u32[]{:S(2)}, u32[]{:S(2)}) collective-permute-start(f32[2,256]{1,0:T(2,128)S(1)} %slice.49), channel_id=1, source_target_pairs={{0,8},{8,16},{16,24},{24,32},{32,40},{40,48},{48,56},{56,64},{64,7... | collective-permute-start | bytes 6152 | tf_op jit(solution)/shard_map/ppermute | solution.py:279
  19.2 6.6 %slice-start = ((s8[6291456]{0:T(1024)(128)(4,1)}), s8[4194304]{0:T(1024)(128)(4,1)S(1)}, s32[]{:S(2)}) async-start(s8[6291456]{0:T(1024)(128)(4,1)} %bitcast.30), calls=%async_computation.3 | async-start | bytes 8388608
  20.0 5.7 %slice-start.1 = ((s8[6291456]{0:T(1024)(128)(4,1)}), s8[2097152]{0:T(1024)(128)(4,1)S(1)}, s32[]{:S(2)}) async-start(s8[6291456]{0:T(1024)(128)(4,1)} %bitcast.30), calls=%async_computation.4 | async-start | bytes 4194304
  20.0 5.7 %copy-start.7 = (bf16[4096,256]{1,0:T(8,128)(2,1)S(1)}, bf16[4096,256]{1,0:T(8,128)(2,1)}, u32[]{:S(2)}) copy-start(bf16[4096,256]{1,0:T(8,128)(2,1)} %param.18) | copy-start | bytes 6291460
  25.8 1.9 copy-start.8
  27.7 2.6 %copy-start.9 = (bf16[128]{0:T(256)(128)(2,1)S(1)}, bf16[128]{0:T(256)(128)(2,1)}, u32[]{:S(2)}) copy-start(bf16[128]{0:T(256)(128)(2,1)} %param.22) | copy-start | bytes 772
  27.7 2.6 %copy-start.4 = (bf16[3,256]{1,0:T(4,128)(2,1)S(1)}, bf16[3,256]{1,0:T(4,128)(2,1)}, u32[]{:S(2)}) copy-start(bf16[3,256]{1,0:T(4,128)(2,1)} %param.17) | copy-start | bytes 4612
  30.5 0.7 copy-start.5
  31.2 1.0 copy-start.1
  184.6 9.3 %all-to-all-start = ((f32[8,1,1536]{2,1,0:T(1,128)}), f32[8,1,1536]{2,1,0:T(1,128)S(1)}, u32[]{:S(2)}, u32[]{:S(2)}) async-start(f32[8,1,1536]{2,1,0:T(1,128)} %broadcast_in_dim.11), calls=%async_computation.1 | async-start | bytes 98304 | tf_op jit(solution)/shard_map/all_to_all | solution.py:284
Sparse Core Ops, SparseCore 0:
  141.7 40.7 reduce-scatter.1

commit v2 on v1

--- a/solution.py
+++ b/solution.py
@@ -33,7 +33,7 @@
     tp = lax.axis_index("tp")
     z, x = sp // 4, sp % 4
     y, c = tp // 2, tp % 2
-    own_pair = 2 * x + c
+    own_pair = x + 4 * c
 
     def device(zz, xx, cc):
         return {"sp": zz * 4 + xx, "tp": y * 2 + cc}
@@ -82,9 +82,9 @@
     for e in range(2):
         head = 2 * c + e
         first.append((k_in.at[:, e * 128 : (e + 1) * 128], k_all.at[sp], p1k_send.at[e], k_recv.at[sp], head, x, z % 2))
-        first.append((q_in.at[e * 128 : (e + 1) * 128], q_own.at[slot_of_sp], q_send.at[e], q_recv.at[slot_of_sp], head, pair_of_sp // 2, pair_of_sp % 2))
+        first.append((q_in.at[e * 128 : (e + 1) * 128], q_own.at[slot_of_sp], q_send.at[e], q_recv.at[slot_of_sp], head, pair_of_sp % 4, pair_of_sp // 4))
         first.append((v_in.at[e * 128 : (e + 1) * 128], v_all.at[sp, pl.ds(0, 128)], p1v_send.at[e], v_recv.at[sp], head, x, z % 2))
-        first.append((lam_in.at[e], lam_own.at[slot_of_sp], l_send.at[e], l_recv.at[slot_of_sp], head, pair_of_sp // 2, pair_of_sp % 2))
+        first.append((lam_in.at[e], lam_own.at[slot_of_sp], l_send.at[e], l_recv.at[slot_of_sp], head, pair_of_sp % 4, pair_of_sp // 4))
     for one in first:
         send(*one)
 
@@ -218,9 +218,8 @@
             n2 = acc[at, 0:128, TQ : 2 * TQ] / acc[at, 128:129, TQ : 2 * TQ]
             diff = n1 - lam * n2
             mean = jnp.mean(diff * diff, axis=0, keepdims=True)
-            o_stage[qb, :, t * TQ : (t + 1) * TQ] = (
-                diff * lax.rsqrt(mean + 1e-05) * gain_ref[...]
-            ).astype(BF16)
+            normed = diff * lax.rsqrt(mean + 1e-05) * gain_ref[...]
+            o_stage[qb, t * TQ : (t + 1) * TQ, :] = normed.T.astype(BF16)
         q_blk = own_pair if qb == 0 else 15 - own_pair
         e = z % 2
         one = (o_stage.at[qb], o_hbm.at[e], o_send.at[qb], o_recv.at[e], q_blk // 4, q_blk % 4, z // 2)
@@ -246,7 +245,7 @@
     hbm = pl.BlockSpec(memory_space=pl.ANY)
     return pl.pallas_call(
         attention_kernel,
-        out_shape=jax.ShapeDtypeStruct((2, 128, TB), BF16),
+        out_shape=jax.ShapeDtypeStruct((2, TB, 128), BF16),
         in_specs=[hbm, hbm, hbm, hbm, pl.BlockSpec(memory_space=pltpu.VMEM)],
         out_specs=hbm,
         scratch_shapes=[
@@ -260,7 +259,7 @@
             pltpu.VMEM((TB, 2 * TQ), F32),
             pltpu.VMEM((2 * NT, VA, 2 * TQ), F32),
             pltpu.VMEM((2 * NT, 1, 2 * TQ), F32),
-            pltpu.VMEM((2, 128, TB), BF16),
+            pltpu.VMEM((2, TB, 128), BF16),
             dma((NB,)), dma((NB,)), dma((2,)), dma((2,)), dma((2,)),
             dma((2,)), dma((2,)), dma((2,)), dma((2,)),
             dma((3,)), dma((3,)), dma((3,)), dma((3,)),
@@ -273,15 +272,157 @@
     )(keys, values_t, query_t, lam, gain)
 
 
+SUB = 2
+HALF = TB // 2
+PR = HALF // SUB
+
+
+def output_kernel(
+    conv_in, attn_in, wc_in, wa_in, gain_ref, out_ref,
+    act, wts, sbuf, rbuf, mix, stats,
+    a_sem, a_recv, a_send, w_sem, w_recv, w_send, r_send, r_recv, t_send, t_recv,
+):
+    sp = lax.axis_index("sp")
+    tp = lax.axis_index("tp")
+    y, c = tp // 2, tp % 2
+
+    def remote(src, dst, send_sem, recv_sem, other):
+        return pltpu.make_async_remote_copy(
+            src_ref=src, dst_ref=dst, send_sem=send_sem, recv_sem=recv_sem,
+            device_id={"sp": sp, "tp": other}, device_id_type=pl.DeviceIdType.MESH,
+        )
+
+    barrier = pltpu.get_barrier_semaphore()
+
+    def greet(i, carry):
+        pl.semaphore_signal(
+            barrier, inc=1, device_id={"sp": sp, "tp": (tp + i) % 8},
+            device_id_type=pl.DeviceIdType.MESH,
+        )
+        return carry
+
+    lax.fori_loop(1, 8, greet, 0)
+
+    partner = y * 2 + (1 - c)
+    local, pairs = [], []
+    sources = [conv_in, attn_in.at[0], attn_in.at[1]]
+    places = [pl.ds(c * 256, 256), pl.ds(512 + c * 256, 128), pl.ds(640 + c * 256, 128)]
+    for n in range(3):
+        dst = act.at[:, places[n]]
+        local.append(pltpu.make_async_copy(sources[n], dst, a_sem.at[n]))
+        pairs.append(remote(sources[n], dst, a_send.at[n], a_recv.at[n], partner))
+    for chunk in range(4):
+        for n, w_in in enumerate((wc_in, wa_in)):
+            dst = wts.at[chunk, pl.ds(n * 512 + c * 256, 256)]
+            k = chunk * 2 + n
+            own = w_in.at[:, pl.ds(chunk * 1024 + c * 512, 512)]
+            theirs = w_in.at[:, pl.ds(chunk * 1024 + (1 - c) * 512, 512)]
+            local.append(pltpu.make_async_copy(own, dst, w_sem.at[k]))
+            pairs.append(remote(theirs, dst, w_send.at[k], w_recv.at[k], partner))
+    for one in local:
+        one.start()
+    pl.semaphore_wait(barrier, 7)
+    for one in pairs:
+        one.start()
+    for one in local:
+        one.wait()
+    for one in pairs:
+        one.wait_recv()
+
+    up, down = ((y + 1) % 4) * 2 + c, ((y + 3) % 4) * 2 + c
+
+    def ring(s, d, u):
+        return remote(
+            sbuf.at[s, d, u], rbuf.at[s, d, u], r_send.at[s, d, u], r_recv.at[s, d, u],
+            up if d == 0 else down,
+        )
+
+    for s in range(4):
+        for u in range(SUB):
+            for d in range(2):
+                chunk = (y + 3 - s) % 4 if d == 0 else (y + 1 + s) % 4
+                first = d * HALF + u * PR
+                part = jnp.dot(
+                    act[first : first + PR, :], wts[chunk], preferred_element_type=F32
+                )
+                if s > 0:
+                    ring(s - 1, d, u).wait_recv()
+                    part = part + rbuf[s - 1, d, u].astype(F32)
+                if s < 3:
+                    sbuf[s, d, u] = part.astype(BF16)
+                    ring(s, d, u).start()
+                else:
+                    mix[first : first + PR, :] = part.astype(BF16)
+
+    ones = jnp.ones((8, 512), BF16)
+    dims = (((1,), (1,)), ((), ()))
+    m = mix[...]
+    square = m.astype(F32) * m.astype(F32)
+    high = square.astype(BF16)
+    low = (square - high.astype(F32)).astype(BF16)
+    total = lax.dot_general(ones, m, dims, preferred_element_type=F32)
+    squares = lax.dot_general(ones, high, dims, preferred_element_type=F32)
+    squares = squares + lax.dot_general(ones, low, dims, preferred_element_type=F32)
+    row = lax.broadcasted_iota(jnp.int32, (8, TB), 0)
+    stats[tp] = jnp.where(row == 0, total, squares)
+
+    def tell(i):
+        return remote(stats.at[tp], stats.at[tp], t_send.at[i - 1], t_recv.at[i - 1], (tp + i) % 8)
+
+    for i in range(1, 8):
+        tell(i).start()
+    for i in range(1, 8):
+        tell(i).wait_recv()
+    everything = stats[0]
+    for n in range(1, 8):
+        everything = everything + stats[n]
+    columns = everything.T
+    mean = columns[:, 0:1] * (1.0 / D)
+    variance = columns[:, 1:2] * (1.0 / D) - mean * mean
+    out_ref[...] = (
+        (mix[...].astype(F32) - mean) * lax.rsqrt(variance + 1e-05) * gain_ref[tp]
+    ).astype(BF16)
+
+    for one in pairs:
+        one.wait_send()
+    for s in range(3):
+        for d in range(2):
+            for u in range(SUB):
+                ring(s, d, u).wait_send()
+    for i in range(1, 8):
+        tell(i).wait_send()
+
+
+def output(conv_out, attn_out, w_conv, w_attn, gain):
+    dma = pltpu.SemaphoreType.DMA
+    hbm = pl.BlockSpec(memory_space=pl.ANY)
+    vmem = pl.BlockSpec(memory_space=pltpu.VMEM)
+    return pl.pallas_call(
+        output_kernel,
+        out_shape=jax.ShapeDtypeStruct((TB, 512), BF16),
+        in_specs=[hbm, hbm, hbm, hbm, vmem],
+        out_specs=vmem,
+        scratch_shapes=[
+            pltpu.VMEM((TB, 1024), BF16),
+            pltpu.VMEM((4, 1024, 512), BF16),
+            pltpu.VMEM((3, 2, SUB, PR, 512), BF16),
+            pltpu.VMEM((3, 2, SUB, PR, 512), BF16),
+            pltpu.VMEM((TB, 512), BF16),
+            pltpu.VMEM((8, 8, TB), F32),
+            dma((3,)), dma((3,)), dma((3,)), dma((8,)), dma((8,)), dma((8,)),
+            dma((3, 2, SUB)), dma((3, 2, SUB)), dma((7,)), dma((7,)),
+        ],
+        compiler_params=pltpu.CompilerParams(
+            collective_id=1, has_side_effects=True, vmem_limit_bytes=48 << 20
+        ),
+        name="output",
+    )(conv_out, attn_out, w_conv, w_attn, gain)
+
+
 def passed_along(block, axis, distance):
     devices = range(lax.axis_size(axis))
     route = [(i - distance, i) for i in devices if i - distance in devices]
     return lax.ppermute(block, axis, route)
-
-
-def copy_for_each(value, axis):
-    copies = jnp.broadcast_to(value, (lax.axis_size(axis), *value.shape))
-    return lax.all_to_all(copies, axis, split_axis=0, concat_axis=0, tiled=True)
 
 
 def per_device(
@@ -330,7 +471,7 @@
 
     lam = jnp.broadcast_to(lambdas[:, None, None], (2, 8, 128))
     gain = head_gain.astype(F32)[:, None]
-    attn_t = attention(keys, values_t, query_t, lam, gain).reshape(256, tok_rows)
+    attn_out = attention(keys, values_t, query_t, lam, gain)
 
     u_b = project(w_conv_b)
     u_c = project(w_conv_c)
@@ -344,19 +485,7 @@
         convolved = convolved + taps_f[tap][None, :] * padded[tap : tap + tok_rows]
     conv_out = (u_b.astype(F32) * convolved).astype(BF16)
 
-    gain_f = out_gain.astype(F32)
-    partial_value = jnp.dot(conv_out, w_out_conv, preferred_element_type=F32) + lax.dot_general(
-        attn_t, w_out_attn, (((0,), (0,)), ((), ())), preferred_element_type=F32
-    )
-    summed = lax.psum_scatter(partial_value.astype(BF16), "tp", scatter_dimension=1, tiled=True)
-    mix_f = summed.astype(F32)
-    width = mix_f.shape[1]
-    stats = jnp.concatenate([jnp.sum(mix_f, axis=-1), jnp.sum(mix_f * mix_f, axis=-1)])
-    total = jnp.sum(copy_for_each(stats, "tp").reshape(lax.axis_size("tp"), -1), axis=0)
-    mean_value = (total[:tok_rows] / D)[:, None]
-    variance = (total[tok_rows:] / D)[:, None] - mean_value * mean_value
-    own_gain = lax.dynamic_slice_in_dim(gain_f, lax.axis_index("tp") * width, width, 0)
-    return ((mix_f - mean_value) * lax.rsqrt(variance + 1e-05) * own_gain[None, :]).astype(BF16)
+    return output(conv_out, attn_out, w_out_conv, w_out_attn, out_gain.astype(F32).reshape(8, 1, 512))
 
 
 def solution(mesh):

time: 204 us -> 159 us (0.78)
  waiting for transfers between devices: 45 us -> 0.01 us
  Pallas kernels: 84.5 us -> 127 us
  matrix products: 42.1 us -> 22.4 us
  between operations: 13.7 us -> 0.37 us
  starting transfers between devices: 8.41 us -> 3.94 us
  other arithmetic: 5.86 us -> 2.02 us
    pallas_call x1 -> x2, Pallas kernels: 84.5 us -> 127 us  [the longest x1 83.4 us: attention(): pl.pallas_call(attention_kernel, out_shape=jax.ShapeDtypeStruct((2, TB, 1...]
    reduce_scatter x1 -> x0, waiting for transfers between devices: 40.9 us -> none  [per_device(): lax.psum_scatter(partial_value.astype(BF16), 'tp', scatter_dimension=1, t...]
    dot_general x2 -> x0, matrix products: 24.9 us -> none  [the longest x1 15.3 us: per_device(): jnp.dot(conv_out, w_out_conv, preferred_element_type=F32)]
    dot_general x3 -> x4, matrix products: 12.8 us -> 18.7 us  [project(): jnp.dot(hidden_states, weight, preferred_element_type=F32).astype(BF16)]
    all_to_all x1 -> x0, starting transfers between devices: 4.49 us -> none  [copy_for_each(): return lax.all_to_all(copies, axis, split_axis=0, concat_axis=0, tiled=True)]
    all_to_all x1 -> x0, waiting for transfers between devices: 4.05 us -> none  [copy_for_each(): return lax.all_to_all(copies, axis, split_axis=0, concat_axis=0, tiled=True)]
    convert_element_type x2 -> x0, other arithmetic: 3.11 us -> none  [the longest x1 2.36 us: per_device(): ((mix_f - mean_value) * lax.rsqrt(variance + 1e-05) * own_gain[None, :])....]
  transfers between devices with their start and end apart: 3 -> 1, of which waited for: 2 -> 0; matrix products, arithmetic and copies ran while one was open for 6% -> 8% of each run, Pallas kernels for 42% -> 52%
where the time goes in v2:
time: 159 us
  Pallas kernels  127 us (80%)
  matrix products  22.4 us (14%)
  starting transfers between devices  3.94 us (2%)
  local copies, waits for them, and re-layouts  3.9 us (2%)
  other arithmetic  2.02 us (1%)
    pallas_call x1, Pallas kernels, attention(): pl.pallas_call(attention_kernel, out_shape=jax.ShapeDtypeStruct((2, TB, 1...  83.4 us
    pallas_call x1, Pallas kernels, output(): pl.pallas_call(output_kernel, out_shape=jax.ShapeDtypeStruct((TB, 512), B...  43.2 us
    dot_general x4, matrix products, project(): jnp.dot(hidden_states, weight, preferred_element_type=F32).astype(BF16)  18.7 us
    ppermute x1, starting transfers between devices, passed_along(): return lax.ppermute(block, axis, route)  3.94 us
    dot_general x2, matrix products, project_t(): lax.dot_general(weight, hidden_states, (((0,), (1,)), ((), ())), preferre...  3.68 us
  transfers between devices with their start and end apart: 1, of which 0 were waited for; matrix products, arithmetic and copies ran while one was open for 8% of the time, Pallas kernels for 52%

profile of v2, /device:TPU:1, one launch (start us, length us, event | category | flops | bytes accessed | tf_op | source)
XLA Modules:
  0.0 159.3 jit_solution(195182363707157100)
XLA Ops:
  0.0 1.6 copy-done
  1.6 5.2 %fusion.2 = f32[768,256]{1,0:T(8,128)S(1)} fusion(bf16[768,4096]{1,0:T(8,128)(2,1)} %param.13, bf16[4096,256]{1,0:T(8,128)(2,1)S(1)} %copy-done), kind=kOutput, calls=%fused_computation.7 | convolution fusion | flops 1611005952 | bytes 9175040 | tf_op jit(solution)/shard_map/dot_general | solution.py:450
  6.9 1.8 %fusion.1 = f32[768,256]{1,0:T(8,128)S(1)} fusion(f32[768,256]{1,0:T(8,128)S(1)} %fusion.2, bf16[768,4096]{1,0:T(8,128)(2,1)S(1)} %copy-done.7, bf16[4096,256]{1,0:T(8,128)(2,1)S(1)} %copy-done.8), kind=kOutput, calls=%fused_computation.5 | convolution fusion | flops 1611202560 | bytes 9961472 | tf_op jit(solution)/shard_map/dot_general | solution.py:450
  8.7 0.0 copy-start.6
  8.7 3.9 %collective-permute-start = (f32[2,256]{1,0:T(2,128)S(1)}, f32[2,256]{1,0:T(2,128)S(1)}, u32[]{:S(2)}, u32[]{:S(2)}) collective-permute-start(f32[2,256]{1,0:T(2,128)S(1)} %slice.41), channel_id=1, source_target_pairs={{0,8},{8,16},{16,24},{24,32},{32,40},{40,48},{48,56},{56,64},{64,7... | collective-permute-start | bytes 6152 | tf_op jit(solution)/shard_map/ppermute | solution.py:425
  12.7 0.0 slice-start
  12.7 0.4 multiply_cosine_fusion.1
  13.1 0.4 fusion.11
  13.6 0.0 slice-start.1
  13.6 0.0 copy-start.9
  13.6 5.6 %convolution_convert_fusion.2 = bf16[768,256]{0,1:T(8,128)(2,1)S(1)} fusion(bf16[768,4096]{1,0:T(8,128)(2,1)} %param.13, bf16[4096,256]{1,0:T(8,128)(2,1)} %param.19), kind=kOutput, calls=%fused_computation.2 | convolution fusion | flops 1610809344 | bytes 8781824 | tf_op jit(solution)/shard_map/dot_general | solution.py:450
  19.2 0.1 convert.20
  19.3 0.0 copy-start.10
  19.3 1.8 %convolution_convert_fusion = bf16[256,768]{1,0:T(8,128)(2,1)S(1)} fusion(bf16[4096,256]{1,0:T(8,128)(2,1)S(1)} %copy-done.9, bf16[768,4096]{1,0:T(8,128)(2,1)S(1)} %bitcast.34), kind=kOutput, calls=%fused_computation | convolution fusion | flops 1610809344 | bytes 8781824 | tf_op jit(solution)/shard_map/dot_general | solution.py:453
  21.2 0.1 convert.21
  21.3 0.0 copy-start.11
  21.3 0.0 copy-start.4
  21.3 1.8 %convolution_convert_fusion.1.v_in = bf16[256,768]{1,0:T(8,128)(2,1)S(1)} fusion(bf16[4096,256]{1,0:T(8,128)(2,1)S(1)} %copy-done.10, bf16[768,4096]{1,0:T(8,128)(2,1)S(1)} %bitcast.34), kind=kOutput, calls=%fused_computation.1 | convolution fusion | flops 1610809344 | bytes 8781824 | tf_op jit(solution)/shard_map/dot_general | solution.py:453
  23.2 0.1 subtract_convert_fusion.1
  23.3 0.0 copy-start.3
  23.3 0.0 copy-start.5
  23.3 0.8 pad_maximum_fusion.1
  24.1 0.1 subtract_convert_fusion
  24.3 1.2 copy.17.k_in
  25.4 0.1 copy.18.gain_ref
  25.6 0.1 broadcast_in_dim.6.lam_in
  25.6 83.4 %attention.1.attn_in = bf16[2,768,128]{2,1,0:T(8,128)(2,1)S(1)} custom-call(bf16[768,256]{1,0:T(8,128)(2,1)S(1)} %copy.17.k_in, bf16[256,768]{1,0:T(8,128)(2,1)S(1)} %convolution_convert_fusion.1.v_in, bf16[256,768]{1,0:T(8,128)(2,1)S(1)} %bitcast.25, f32[2,8,128]{2,1,0:T(8,128)S(1)} %broadcast_in_dim.6.lam_in, f32[128,1]{1,0:T(8,128)S(1)} %copy.18.gain_ref), custom_call_target="tpu_custom_call" | custom-call | tf_op jit(solution)/shard_map/attention/pallas_call | solution.py:246
  109.1 0.0 copy-start.1
  109.1 0.0 copy-start.2
  109.1 6.0 %fusion.9.conv_in = bf16[768,256]{1,0:T(8,128)(2,1)S(1)} fusion(f32[2,256]{1,0:T(2,128)S(1)} %collective-permute-done, f32[768,256]{1,0:T(8,128)} %copy-done.6, f32[256]{0:T(256)S(1)} %bitcast.32, f32[256]{0:T(256)S(1)} %bitcast.31, f32[256]{0:T(256)S(1)} %bitcast.30, bf16[768,4096]{1,0:T(8,128)(2,1)} %param.13, bf16[4096,256]{1,0:T(8,128)(2,1)} %param.14), kind=kOutput, calls=%fused_computation.17 | convolution fusion | flops 1612775424 | bytes 9573376 | tf_op jit(solution)/shard_map/dot_general | solution.py:450
  115.2 43.2 %output.1 = bf16[768,512]{1,0:T(8,128)(2,1)S(1)} custom-call(bf16[768,256]{1,0:T(8,128)(2,1)S(1)} %fusion.9.conv_in, bf16[2,768,128]{2,1,0:T(8,128)(2,1)S(1)} %attention.1.attn_in, bf16[256,4096]{1,0:T(8,128)(2,1)S(1)} %copy-done.1, bf16[256,4096]{1,0:T(8,128)(2,1)S(1)} %copy-done.2, f32[8,1,512]{2,1,0:T(1,128)S(1)} %bitcast.26), custom_call_target="tpu_custom_call" | custom-call | tf_op jit(solution)/shard_map/output/pallas_call | solution.py:400
  158.4 0.9 copy.20
  (25 shorter events, 0.1 us)
Async XLA Ops:
  0.0 1.6 copy-start
  0.0 6.8 %copy-start.7 = (bf16[768,4096]{1,0:T(8,128)(2,1)S(1)}, bf16[768,4096]{1,0:T(8,128)(2,1)}, u32[]{:S(2)}) copy-start(bf16[768,4096]{1,0:T(8,128)(2,1)} %param.13) | copy-start | bytes 18874372
  0.0 6.9 %copy-start.8 = (bf16[4096,256]{1,0:T(8,128)(2,1)S(1)}, bf16[4096,256]{1,0:T(8,128)(2,1)}, u32[]{:S(2)}) copy-start(bf16[4096,256]{1,0:T(8,128)(2,1)} %param.16) | copy-start | bytes 6291460
  8.7 4.0 %copy-start.6 = (f32[768,256]{1,0:T(8,128)}, f32[768,256]{1,0:T(8,128)S(1)}, u32[]{:S(2)}) copy-start(f32[768,256]{1,0:T(8,128)S(1)} %fusion.1) | copy-start | bytes 2359300
  8.7 100.4 %collective-permute-start = (f32[2,256]{1,0:T(2,128)S(1)}, f32[2,256]{1,0:T(2,128)S(1)}, u32[]{:S(2)}, u32[]{:S(2)}) collective-permute-start(f32[2,256]{1,0:T(2,128)S(1)} %slice.41), channel_id=1, source_target_pairs={{0,8},{8,16},{16,24},{24,32},{32,40},{40,48},{48,56},{56,64},{64,7... | collective-permute-start | bytes 6152 | tf_op jit(solution)/shard_map/ppermute | solution.py:425
  12.7 6.6 %slice-start = ((s8[6291456]{0:T(1024)(128)(4,1)}), s8[4194304]{0:T(1024)(128)(4,1)S(1)}, s32[]{:S(2)}) async-start(s8[6291456]{0:T(1024)(128)(4,1)} %bitcast.33), calls=%async_computation | async-start | bytes 8388608
  13.6 5.7 %slice-start.1 = ((s8[6291456]{0:T(1024)(128)(4,1)}), s8[2097152]{0:T(1024)(128)(4,1)S(1)}, s32[]{:S(2)}) async-start(s8[6291456]{0:T(1024)(128)(4,1)} %bitcast.33), calls=%async_computation.1 | async-start | bytes 4194304
  13.6 5.7 %copy-start.9 = (bf16[4096,256]{1,0:T(8,128)(2,1)S(1)}, bf16[4096,256]{1,0:T(8,128)(2,1)}, u32[]{:S(2)}) copy-start(bf16[4096,256]{1,0:T(8,128)(2,1)} %param.18) | copy-start | bytes 6291460
  19.3 1.9 %copy-start.10 = (bf16[4096,256]{1,0:T(8,128)(2,1)S(1)}, bf16[4096,256]{1,0:T(8,128)(2,1)}, u32[]{:S(2)}) copy-start(bf16[4096,256]{1,0:T(8,128)(2,1)} %param.20) | copy-start | bytes 6291460
  21.3 1.9 %copy-start.11 = (bf16[128]{0:T(256)(128)(2,1)S(1)}, bf16[128]{0:T(256)(128)(2,1)}, u32[]{:S(2)}) copy-start(bf16[128]{0:T(256)(128)(2,1)} %param.22) | copy-start | bytes 772
  21.3 1.9 %copy-start.4 = (bf16[3,256]{1,0:T(4,128)(2,1)S(1)}, bf16[3,256]{1,0:T(4,128)(2,1)}, u32[]{:S(2)}) copy-start(bf16[3,256]{1,0:T(4,128)(2,1)} %param.17) | copy-start | bytes 4612
  23.3 2.2 %copy-start.3 = (bf16[4096]{0:T(1024)(128)(2,1)S(1)}, bf16[4096]{0:T(1024)(128)(2,1)}, u32[]{:S(2)}) copy-start(bf16[4096]{0:T(1024)(128)(2,1)} %param.25) | copy-start | bytes 24580
  23.3 2.2 %copy-start.5 = (f32[2]{0:T(128)S(1)}, f32[2]{0:T(128)}, u32[]{:S(2)}) copy-start(f32[2]{0:T(128)} %param.21) | copy-start | bytes 28
  109.1 6.1 %copy-start.1 = (bf16[256,4096]{1,0:T(8,128)(2,1)S(1)}, bf16[256,4096]{1,0:T(8,128)(2,1)}, u32[]{:S(2)}) copy-start(bf16[256,4096]{1,0:T(8,128)(2,1)} %wc_in.1) | copy-start | bytes 6291460
  109.1 6.1 %copy-start.2 = (bf16[256,4096]{1,0:T(8,128)(2,1)S(1)}, bf16[256,4096]{1,0:T(8,128)(2,1)}, u32[]{:S(2)}) copy-start(bf16[256,4096]{1,0:T(8,128)(2,1)} %wa_in.1) | copy-start | bytes 6291460

commit v3 on v1

v3 whole, which is shorter than its diff:
```python
import jax
import jax.numpy as jnp
from jax import lax
from jax.experimental import pallas as pl
from jax.experimental.pallas import tpu as pltpu
from jax.sharding import PartitionSpec as P

D = 4096
QK = 64
TAPS = 3
TB = 768
NB = 16
TQ = 256
NT = TB // TQ
VA = 144
SUB = 2
HALF = TB // 2
PR = HALF // SUB
LOG2E = 1.4426950408889634
NEG_LARGE = -1e30
BF16 = jnp.bfloat16
F32 = jnp.float32


def mixer_kernel(
    hid_in, wk_in, wv_in, wq_in, wb_in, wc_in, wh_in, oc_in, oa_in,
    lam_in, hgain_ref, cs_ref, taps_ref, ogain_ref,
    out_ref,
    hid, wp, k_own, v_own, q_src, gated, rim, u_b,
    k_all, v_all, q_own, qa, lam_own, s0, s1, s2, acc, m_ref, o_stage,
    act, wts, sbuf, rbuf, mix, stats,
    h_sem, w_sem, ow_sem, ow_send, ow_recv, rim_send, rim_recv,
    k_recv, v_recv, q_recv, l_recv, o_recv,
    q_send, l_send, p1k_send, p1v_send, rk_send, rv_send, lk_send, lv_send,
    dk_send, dv_send, o_send,
    c_send, c_recv, f_send, f_recv, r_send, r_recv, t_send, t_recv,
):
    sp = lax.axis_index("sp")
    tp = lax.axis_index("tp")
    z, x = sp // 4, sp % 4
    y, c = tp // 2, tp % 2
    own_pair = x + 4 * c
    left, right = (x + 3) % 4, (x + 1) % 4

    def copy_to(src, dst, send_sem, recv_sem, at_sp, at_tp):
        return pltpu.make_async_remote_copy(
            src_ref=src, dst_ref=dst, send_sem=send_sem, recv_sem=recv_sem,
            device_id={"sp": at_sp, "tp": at_tp}, device_id_type=pl.DeviceIdType.MESH,
        )

    def remote(src, dst, send_sem, recv_sem, zz, xx, cc):
        return copy_to(src, dst, send_sem, recv_sem, zz * 4 + xx, y * 2 + cc)

    def partner(src, dst, send_sem, recv_sem):
        return copy_to(src, dst, send_sem, recv_sem, sp, y * 2 + (1 - c))

    loads = [pltpu.make_async_copy(wk_in, wp.at[0], w_sem.at[0])]
    for m in range(NT):
        loads.append(pltpu.make_async_copy(hid_in.at[m * TQ : (m + 1) * TQ], hid.at[m], h_sem.at[m]))
    for n, w_in in enumerate((wv_in, wq_in, wc_in, wh_in, wb_in)):
        loads.append(pltpu.make_async_copy(w_in, wp.at[n + 1], w_sem.at[n + 1]))
    own_out, pair_out = [], []
    for chunk in range(4):
        for n, w_in in enumerate((oc_in, oa_in)):
            dst = wts.at[chunk, pl.ds(n * 512 + c * 256, 256)]
            k = chunk * 2 + n
            own = w_in.at[:, pl.ds(chunk * 1024 + c * 512, 512)]
            theirs = w_in.at[:, pl.ds(chunk * 1024 + (1 - c) * 512, 512)]
            own_out.append(pltpu.make_async_copy(own, dst, ow_sem.at[k]))
            pair_out.append(partner(theirs, dst, ow_send.at[k], ow_recv.at[k]))
    for one in loads:
        one.start()

    barrier = pltpu.get_barrier_semaphore()
    me = sp * 2 + c

    def greet_plane(i, carry):
        other = (me + i) % 32
        pl.semaphore_signal(
            barrier, inc=1, device_id={"sp": other // 2, "tp": y * 2 + other % 2},
            device_id_type=pl.DeviceIdType.MESH,
        )
        return carry

    def greet_column(i, carry):
        pl.semaphore_signal(
            barrier, inc=1, device_id={"sp": sp, "tp": ((y + 1) * 2 + i) % 8},
            device_id_type=pl.DeviceIdType.MESH,
        )
        return carry

    lax.fori_loop(1, 32, greet_plane, 0)
    lax.fori_loop(0, 6, greet_column, 0)

    def project(m, n):
        r = jnp.dot(hid[m], wp[n], preferred_element_type=F32)
        return r.astype(BF16).astype(F32)

    def rotated(t, m, scale):
        cos, sin = cs_ref[0, m], cs_ref[1, m]
        if scale is not None:
            cos, sin = cos * scale, sin * scale
        parts = []
        for g in range(4):
            a, b = t[g * 64 : g * 64 + 32], t[g * 64 + 32 : g * 64 + 64]
            parts += [a * cos - b * sin, b * cos + a * sin]
        return jnp.concatenate(parts, axis=0)

    loads[0].wait()

    def key_rows(m, carry):
        pltpu.make_async_copy(hid_in.at[0:TQ], hid.at[m], h_sem.at[m]).wait()
        r = rotated(project(m, 0).T, m, None).T.astype(BF16)
        rows = pl.ds(pl.multiple_of(m * TQ, TQ), TQ)
        k_own[0, rows, :] = r[:, 0:128]
        k_own[1, rows, :] = r[:, 128:256]
        return carry

    lax.fori_loop(0, NT, key_rows, 0)
    pl.semaphore_wait(barrier, 37)
    for one in own_out + pair_out:
        one.start()

    pair_of_sp = jnp.where(sp < 8, sp, 15 - sp)
    slot_of_sp = jnp.where(sp < 8, 0, 1)

    def kv_same(e):
        return (2 * c + e == z) & (z % 2 == c)

    def q_same(e):
        return (2 * c + e == z) & (pair_of_sp % 4 == x) & (pair_of_sp // 4 == c)

    def key_first(e):
        return remote(k_own.at[e], k_all.at[sp], p1k_send.at[e], k_recv.at[sp], 2 * c + e, x, z % 2)

    def value_first(e):
        return remote(v_own.at[e], v_all.at[sp, pl.ds(0, 128)], p1v_send.at[e], v_recv.at[sp], 2 * c + e, x, z % 2)

    def query_first(e):
        return remote(q_src.at[e], q_own.at[slot_of_sp], q_send.at[e], q_recv.at[slot_of_sp], 2 * c + e, pair_of_sp % 4, pair_of_sp // 4)

    def lam_first(e):
        return remote(lam_in.at[e], lam_own.at[slot_of_sp], l_send.at[e], l_recv.at[slot_of_sp], 2 * c + e, pair_of_sp % 4, pair_of_sp // 4)

    def unless(same, action):
        @pl.when(jnp.logical_not(same))
        def _():
            action()

    for e in range(2):
        unless(kv_same(e), lambda: key_first(e).start())

        @pl.when(kv_same(e))
        def _():
            k_all[sp] = k_own[e]

    def column(m):
        return pl.ds(pl.multiple_of(m * TQ, TQ), TQ)

    loads[4].wait()

    def value_rows(m, carry):
        r = project(m, 1).T.astype(BF16)
        v_own[0, :, column(m)] = r[0:128]
        v_own[1, :, column(m)] = r[128:256]
        return carry

    lax.fori_loop(0, NT, value_rows, 0)
    for e in range(2):
        unless(kv_same(e), lambda: value_first(e).start())

        @pl.when(kv_same(e))
        def _():
            v_all[sp, 0:128, :] = v_own[e]

    loads[5].wait()

    def query_rows(m, carry):
        r = rotated(project(m, 2).T, m, LOG2E * QK ** (-0.5)).astype(BF16)
        q_src[0, :, column(m)] = r[0:128]
        q_src[1, :, column(m)] = r[128:256]
        return carry

    lax.fori_loop(0, NT, query_rows, 0)
    for e in range(2):
        unless(q_same(e), lambda: query_first(e).start())
        unless(q_same(e), lambda: lam_first(e).start())

        @pl.when(q_same(e))
        def _():
            q_own[slot_of_sp] = q_src[e]
            lam_own[slot_of_sp] = lam_in[e]

    for n in (6, 7, 8):
        loads[n].wait()

    def gated_rows(m, carry):
        gated[pl.ds(pl.multiple_of(8 + m * TQ, 8), TQ), :] = project(m, 3) * project(m, 4)
        return carry

    lax.fori_loop(0, NT, gated_rows, 0)

    def gate_rows(m, carry):
        u_b[m] = jnp.dot(hid[m], wp[5], preferred_element_type=F32).astype(BF16)
        return carry

    lax.fori_loop(0, NT, gate_rows, 0)

    rim_copy = copy_to(
        gated.at[pl.ds(TB, 8)], rim, rim_send, rim_recv, (sp + 1) % 16, tp
    )

    @pl.when(sp < 15)
    def _():
        rim_copy.start()

    def ones(j, carry):
        v_all[j, 128:VA, :] = jnp.ones((VA - 128, TB), BF16)
        return carry

    lax.fori_loop(0, NB, ones, 0)
    acc[...] = jnp.zeros(acc.shape, F32)
    m_ref[...] = jnp.full(m_ref.shape, NEG_LARGE, F32)

    @pl.when(sp > 0)
    def _():
        rim_copy.wait_recv()
        gated[0:8, :] = rim[...]

    @pl.when(sp == 0)
    def _():
        gated[0:8, :] = jnp.zeros((8, 256), F32)

    for m in range(NT):
        total = jnp.zeros((TQ, 256), F32)
        for tap in range(TAPS):
            first = 8 + m * TQ - (TAPS - 1) + tap
            total = total + taps_ref[tap : tap + 1, :] * gated[first : first + TQ, :]
        conv = (u_b[m].astype(F32) * total).astype(BF16)
        act[2 * c, m * TQ : (m + 1) * TQ, :] = conv[:, 0:128]
        act[2 * c + 1, m * TQ : (m + 1) * TQ, :] = conv[:, 128:256]

    zero = jnp.zeros((QK, TQ), BF16)
    for qb in range(2):
        q_blk = own_pair if qb == 0 else 15 - own_pair
        same = (q_blk == sp) & (z // 2 == c)
        unless(same, lambda: remote(q_src.at[0], q_own.at[qb], q_send.at[0], q_recv.at[qb], z, x, 1 - c).wait_recv())
        unless(same, lambda: remote(lam_in.at[0], lam_own.at[qb], l_send.at[0], l_recv.at[qb], z, x, 1 - c).wait_recv())
        for t in range(NT):
            qt = q_own[qb, :, t * TQ : (t + 1) * TQ]
            qa[qb * NT + t, 0:QK, 0:TQ] = qt[0:QK]
            qa[qb * NT + t, QK:128, 0:TQ] = zero
            qa[qb * NT + t, 0:QK, TQ : 2 * TQ] = zero
            qa[qb * NT + t, QK:128, TQ : 2 * TQ] = qt[QK:128]

    conv_sends = []
    for n in range(2):
        piece = act.at[2 * c + n]
        conv_sends.append(partner(piece, piece, c_send.at[n], c_recv.at[n]))
    for one in conv_sends:
        one.start()

    scores = (s0, s1, s2)

    def unit(qb, j, diagonal):
        tops = [None] * NT

        def produce(t):
            rows = TQ * (t + 1) if diagonal else TB
            s = jnp.dot(k_all[j, 0:rows, :], qa[qb * NT + t], preferred_element_type=F32)
            if diagonal:
                key = lax.broadcasted_iota(jnp.int32, (rows, 2 * TQ), 0)
                query = lax.broadcasted_iota(jnp.int32, (rows, 2 * TQ), 1)
                query = jnp.where(query >= TQ, query - TQ, query) + t * TQ
                s = jnp.where(key <= query, s, NEG_LARGE)
            scores[t][0:rows, :] = s
            tops[t] = jnp.max(s, axis=0, keepdims=True)

        def consume(t):
            rows = TQ * (t + 1) if diagonal else TB
            at = qb * NT + t
            before = m_ref[at]
            after = jnp.maximum(before, tops[t])
            w = jnp.exp2(scores[t][0:rows, :] - after).astype(BF16)
            factor = jnp.exp2(before - after)
            acc[at] = acc[at] * factor + jnp.dot(
                v_all[j, :, 0:rows], w, preferred_element_type=F32
            )
            m_ref[at] = after

        produce(0)
        produce(1)
        consume(0)
        produce(2)
        consume(1)
        consume(2)

    def k_copy(blk, sems, n, xx, cc):
        return remote(k_all.at[blk], k_all.at[blk], sems.at[n], k_recv.at[blk], z, xx, cc)

    def v_copy(blk, sems, n, xx, cc):
        part = v_all.at[blk, pl.ds(0, 128)]
        return remote(part, part, sems.at[n], v_recv.at[blk], z, xx, cc)

    def block_of(w, u):
        side = jnp.where(u < 2, left, right)
        col = jnp.where(w == 0, x, jnp.where(w == 3, (x + 2) % 4, side))
        row = jnp.where(w == 2, (u + 2) % 4, u)
        return row * 4 + col

    def arrived(blk):
        k_copy(blk, dk_send, 0, x, 1 - c).wait_recv()
        v_copy(blk, dv_send, 0, x, 1 - c).wait_recv()

    def pass_right(blk, n):
        k_copy(blk, rk_send, n, right, c).start()
        v_copy(blk, rv_send, n, right, c).start()

    def pass_left(blk, n):
        k_copy(blk, lk_send, n, left, c).start()
        v_copy(blk, lv_send, n, left, c).start()

    def pass_partner(blk, n):
        k_copy(blk, dk_send, n, x, 1 - c).start()
        v_copy(blk, dv_send, n, x, 1 - c).start()

    low, high = c * 4 + x, (c + 2) * 4 + x
    unless((low == sp) & (z // 2 == c), lambda: arrived(low))
    pass_right(low, 0)
    unless((high == sp) & (z // 2 == c), lambda: arrived(high))
    pass_left(high, 0)
    pass_right(high, 1)
    pass_left(low, 1)
    pass_partner(low, 0)
    pass_partner(high, 1)

    def exchange(w):
        from_left, from_right = block_of(w, c), block_of(w, c + 2)
        arrived(from_left)

        @pl.when(w == 1)
        def _():
            pass_right(from_left, 2)

        pass_partner(from_left, 2 * w)
        arrived(from_right)

        @pl.when(w == 1)
        def _():
            pass_left(from_right, 2)

        pass_partner(from_right, 2 * w + 1)

    def step(i, carry):
        w, k = i // 4, i % 4
        u = jnp.where(k < 2, c + 2 * k, 1 - c + 2 * (k - 2))
        blk = block_of(w, u)

        @pl.when((k == 3) & (w < 3))
        def _():
            exchange(w + 1)

        @pl.when(k >= 2)
        def _():
            arrived(blk)

        def for_queries(qb, carry):
            q_blk = jnp.where(qb == 0, own_pair, 15 - own_pair)

            @pl.when(blk < q_blk)
            def _():
                unit(qb, blk, False)

            @pl.when(blk == q_blk)
            def _():
                unit(qb, blk, True)

            return carry

        lax.fori_loop(0, 2, for_queries, 0)
        return carry

    lax.fori_loop(0, NB, step, 0)

    def out_same(q_blk):
        return (q_blk == sp) & (z // 2 == c)

    def out_copy(qb, q_blk):
        return remote(
            o_stage.at[qb], act.at[4 + z], o_send.at[qb], o_recv.at[z % 2],
            q_blk // 4, q_blk % 4, z // 2,
        )

    q_blks = (own_pair, 15 - own_pair)
    for qb in range(2):
        lam = lam_own[qb, 0:1, 0:1]
        for t in range(NT):
            at = qb * NT + t
            n1 = acc[at, 0:128, 0:TQ] / acc[at, 128:129, 0:TQ]
            n2 = acc[at, 0:128, TQ : 2 * TQ] / acc[at, 128:129, TQ : 2 * TQ]
            diff = n1 - lam * n2
            mean = jnp.mean(diff * diff, axis=0, keepdims=True)
            normed = diff * lax.rsqrt(mean + 1e-05) * hgain_ref[...]
            o_stage[qb, t * TQ : (t + 1) * TQ, :] = normed.T.astype(BF16)
        unless(out_same(q_blks[qb]), lambda: out_copy(qb, q_blks[qb]).start())

        @pl.when(out_same(q_blks[qb]))
        def _():
            act[4 + z] = o_stage[qb]

    forwards = []
    for e in range(2):
        head = 2 * c + e
        made_here = (head == z) & ((sp == own_pair) | (sp == 15 - own_pair))
        piece = act.at[4 + head]
        unless(made_here, lambda: remote(o_stage.at[0], piece, o_send.at[0], o_recv.at[e], z, x, 1 - c).wait_recv())
        forwards.append(partner(piece, piece, f_send.at[e], f_recv.at[e]))
        forwards[e].start()
    for one in own_out:
        one.wait()
    for one in pair_out + conv_sends + forwards:
        one.wait_recv()

    up, down = ((y + 1) % 4) * 2 + c, ((y + 3) % 4) * 2 + c

    def ring(s, d, u):
        return copy_to(
            sbuf.at[s, d, u], rbuf.at[s, d, u], r_send.at[s, d, u], r_recv.at[s, d, u],
            sp, up if d == 0 else down,
        )

    for s in range(4):
        for u in range(SUB):
            for d in range(2):
                chunk = (y + 3 - s) % 4 if d == 0 else (y + 1 + s) % 4
                first = d * HALF + u * PR
                rows = jnp.concatenate([act[n, first : first + PR, :] for n in range(8)], axis=1)
                part = jnp.dot(rows, wts[chunk], preferred_element_type=F32)
                if s > 0:
                    ring(s - 1, d, u).wait_recv()
                    part = part + rbuf[s - 1, d, u].astype(F32)
                if s < 3:
                    sbuf[s, d, u] = part.astype(BF16)
                    ring(s, d, u).start()
                else:
                    mix[first : first + PR, :] = part.astype(BF16)

    ones_row = jnp.ones((8, 512), BF16)
    dims = (((1,), (1,)), ((), ()))
    m = mix[...]
    square = m.astype(F32) * m.astype(F32)
    high = square.astype(BF16)
    low = (square - high.astype(F32)).astype(BF16)
    total = lax.dot_general(ones_row, m, dims, preferred_element_type=F32)
    squares = lax.dot_general(ones_row, high, dims, preferred_element_type=F32)
    squares = squares + lax.dot_general(ones_row, low, dims, preferred_element_type=F32)
    row = lax.broadcasted_iota(jnp.int32, (8, TB), 0)
    stats[tp] = jnp.where(row == 0, total, squares)

    def tell(i):
        return copy_to(stats.at[tp], stats.at[tp], t_send.at[i - 1], t_recv.at[i - 1], sp, (tp + i) % 8)

    for i in range(1, 8):
        tell(i).start()
    for i in range(1, 8):
        tell(i).wait_recv()
    everything = stats[0]
    for n in range(1, 8):
        everything = everything + stats[n]
    columns = everything.T
    mean = columns[:, 0:1] * (1.0 / D)
    variance = columns[:, 1:2] * (1.0 / D) - mean * mean
    out_ref[...] = (
        (mix[...].astype(F32) - mean) * lax.rsqrt(variance + 1e-05) * ogain_ref[tp]
    ).astype(BF16)


    for e in range(2):
        unless(kv_same(e), lambda: key_first(e).wait_send())
        unless(kv_same(e), lambda: value_first(e).wait_send())
        unless(q_same(e), lambda: query_first(e).wait_send())
        unless(q_same(e), lambda: lam_first(e).wait_send())
        unless(out_same(q_blks[e]), lambda: out_copy(e, q_blks[e]).wait_send())

    @pl.when(sp < 15)
    def _():
        rim_copy.wait_send()

    for n in range(3):
        k_copy(0, rk_send, n, right, c).wait_send()
        v_copy(0, rv_send, n, right, c).wait_send()
        k_copy(0, lk_send, n, left, c).wait_send()
        v_copy(0, lv_send, n, left, c).wait_send()
    for n in range(8):
        k_copy(0, dk_send, n, x, 1 - c).wait_send()
        v_copy(0, dv_send, n, x, 1 - c).wait_send()
    for one in pair_out + conv_sends + forwards:
        one.wait_send()
    for s in range(3):
        for d in range(2):
            for u in range(SUB):
                ring(s, d, u).wait_send()
    for i in range(1, 8):
        tell(i).wait_send()


def mixer(*arrays):
    dma = pltpu.SemaphoreType.DMA
    hbm = pl.BlockSpec(memory_space=pl.ANY)
    vmem = pl.BlockSpec(memory_space=pltpu.VMEM)
    return pl.pallas_call(
        mixer_kernel,
        out_shape=jax.ShapeDtypeStruct((TB, 512), BF16),
        in_specs=[hbm] * 9 + [vmem] * 5,
        out_specs=vmem,
        scratch_shapes=[
            pltpu.VMEM((NT, TQ, D), BF16),
            pltpu.VMEM((6, D, 256), BF16),
            pltpu.VMEM((2, TB, 128), BF16),
            pltpu.VMEM((2, 128, TB), BF16),
            pltpu.VMEM((2, 128, TB), BF16),
            pltpu.VMEM((TB + 8, 256), F32),
            pltpu.VMEM((8, 256), F32),
            pltpu.VMEM((NT, TQ, 256), BF16),
            pltpu.VMEM((NB, TB, 128), BF16),
            pltpu.VMEM((NB, VA, TB), BF16),
            pltpu.VMEM((2, 128, TB), BF16),
            pltpu.VMEM((2 * NT, 128, 2 * TQ), BF16),
            pltpu.VMEM((2, 8, 128), F32),
            pltpu.VMEM((TB, 2 * TQ), F32),
            pltpu.VMEM((TB, 2 * TQ), F32),
            pltpu.VMEM((TB, 2 * TQ), F32),
            pltpu.VMEM((2 * NT, VA, 2 * TQ), F32),
            pltpu.VMEM((2 * NT, 1, 2 * TQ), F32),
            pltpu.VMEM((2, TB, 128), BF16),
            pltpu.VMEM((8, TB, 128), BF16),
            pltpu.VMEM((4, 1024, 512), BF16),
            pltpu.VMEM((3, 2, SUB, PR, 512), BF16),
            pltpu.VMEM((3, 2, SUB, PR, 512), BF16),
            pltpu.VMEM((TB, 512), BF16),
            pltpu.VMEM((8, 8, TB), F32),
            dma((NT,)), dma((6,)), dma((8,)), dma((8,)), dma((8,)), dma, dma,
            dma((NB,)), dma((NB,)), dma((2,)), dma((2,)), dma((2,)),
            dma((2,)), dma((2,)), dma((2,)), dma((2,)),
            dma((3,)), dma((3,)), dma((3,)), dma((3,)),
            dma((8,)), dma((8,)), dma((2,)),
            dma((2,)), dma((2,)), dma((2,)), dma((2,)),
            dma((3, 2, SUB)), dma((3, 2, SUB)), dma((7,)), dma((7,)),
        ],
        compiler_params=pltpu.CompilerParams(
            collective_id=0, has_side_effects=True, vmem_limit_bytes=67043328
        ),
        name="mixer",
    )(*arrays)


def per_device(
    hidden_states,
    w_conv_b,
    w_conv_c,
    w_conv_h,
    conv_taps,
    w_query,
    w_key,
    w_value,
    lambdas,
    head_gain,
    w_out_conv,
    w_out_attn,
    out_gain,
):
    first = lax.axis_index("sp") * TB
    positions = (first + jnp.arange(TB, dtype=jnp.int32)).astype(F32).reshape(NT, 1, TQ)
    inverse = 1.0 / 10000.0 ** (jnp.arange(0, QK, 2, dtype=F32) / QK)
    angles = positions * inverse[None, :, None]
    table = jnp.stack([jnp.cos(angles), jnp.sin(angles)])
    return mixer(
        hidden_states, w_key, w_value, w_query, w_conv_b, w_conv_c, w_conv_h,
        w_out_conv, w_out_attn,
        jnp.broadcast_to(lambdas[:, None, None], (2, 8, 128)),
        head_gain.astype(F32)[:, None],
        table,
        conv_taps.astype(F32),
        out_gain.astype(F32).reshape(8, 1, 512),
    )


def solution(mesh):
    return jax.shard_map(
        per_device,
        mesh=mesh,
        in_specs=(
            P("sp", None),
            P(None, "tp"),
            P(None, "tp"),
            P(None, "tp"),
            P(None, "tp"),
            P(None, "tp"),
            P(None, "tp"),
            P(None, "tp"),
            P("tp"),
            P(),
            P("tp", None),
            P("tp", None),
            P(),
        ),
        out_specs=P("sp", "tp"),
        check_vma=False,
    )
```

time: 204 us -> 117 us (0.57)
  waiting for transfers between devices: 45 us -> 0 us
  matrix products: 42.1 us -> 0 us
  Pallas kernels: 84.5 us -> 107 us
  between operations: 13.7 us -> 0.02 us
  starting transfers between devices: 8.41 us -> 0 us
    dot_general x7 -> x0, matrix products: 42.1 us -> none  [the longest x1 15.3 us: per_device(): jnp.dot(conv_out, w_out_conv, preferred_element_type=F32)]
    reduce_scatter x1 -> x0, waiting for transfers between devices: 40.9 us -> none  [per_device(): lax.psum_scatter(partial_value.astype(BF16), 'tp', scatter_dimension=1, t...]
    pallas_call x1, Pallas kernels: 84.5 us -> 107 us  [mixer(): pl.pallas_call(mixer_kernel, out_shape=jax.ShapeDtypeStruct((TB, 512), BF...]
    all_to_all x1 -> x0, starting transfers between devices: 4.49 us -> none  [copy_for_each(): return lax.all_to_all(copies, axis, split_axis=0, concat_axis=0, tiled=True)]
    all_to_all x1 -> x0, waiting for transfers between devices: 4.05 us -> none  [copy_for_each(): return lax.all_to_all(copies, axis, split_axis=0, concat_axis=0, tiled=True)]
    ppermute x1 -> x0, starting transfers between devices: 3.92 us -> none  [passed_along(): return lax.ppermute(block, axis, route)]
  transfers between devices with their start and end apart: 3 -> 0, of which waited for: 2 -> 0; matrix products, arithmetic and copies ran while one was open for 6% -> 0% of each run, Pallas kernels for 42% -> 0%
where the time goes in v3:
time: 117 us; the launch traced here: 116 us
  Pallas kernels  107 us (91%)
  other arithmetic  4.36 us (4%)
  local copies, waits for them, and re-layouts  4.12 us (4%)
    pallas_call x1, Pallas kernels, mixer(): pl.pallas_call(mixer_kernel, out_shape=jax.ShapeDtypeStruct((TB, 512), BF...  107 us

profile of v3, /device:TPU:1, one launch (start us, length us, event | category | flops | bytes accessed | tf_op | source)
XLA Modules:
  0.0 115.6 jit_solution(2222355719171496239)
XLA Ops:
  0.0 0.7 bitcast_convert_fusion
  0.7 1.3 %convert_element_type.13.taps_ref = f32[3,256]{1,0:T(4,128)} convert(bf16[3,256]{1,0:T(4,128)(2,1)} %param.17) | non-fusion elementwise | flops 768 | bytes 4608 | tf_op jit(solution)/shard_map/convert_element_type | solution.py:583
  2.0 1.3 %broadcast_in_dim.12.lam_in = f32[2,8,128]{2,1,0:T(8,128)} broadcast(f32[2]{0:T(128)} %param.21), dimensions={0} | broadcast | bytes 8200 | tf_op jit(solution)/shard_map/broadcast_in_dim | solution.py:580
  3.3 1.3 %reshape.34 = f32[4096]{0:T(1024)} convert(bf16[4096]{0:T(1024)(128)(2,1)} %param.25) | non-fusion elementwise | flops 4096 | bytes 24576 | tf_op jit(solution)/shard_map/reshape | solution.py:584
  4.6 0.7 copy.14.hgain_ref
  5.3 0.4 multiply_cosine_fusion
  5.7 0.7 pad_maximum_fusion.cs_ref
  6.4 107.1 %mixer.1 = bf16[768,512]{1,0:T(8,128)(2,1)} custom-call(bf16[768,4096]{1,0:T(8,128)(2,1)} %hid_in.1, bf16[4096,256]{1,0:T(8,128)(2,1)} %wk_in.1, bf16[4096,256]{1,0:T(8,128)(2,1)} %wv_in.1, bf16[4096,256]{1,0:T(8,128)(2,1)} %wq_in.1, bf16[4096,256]{1,0:T(8,128)(2,1)} %wb_in.1, bf16[4096,256]{1,0:T(8,128)(2,1)} %wc_in.1, bf16[4096,256]{1,0:T(8,128)(2,1)} %wh_in.1, ...), custom_call_target="tpu_custom_call" | custom-call | tf_op jit(solution)/shard_map/mixer/pallas_call | solution.py:511
  113.5 2.1 %copy.16 = bf16[768,512]{1,0:T(8,128)(2,1)} copy(bf16[768,512]{1,0:T(8,128)(2,1)} %mixer.1) | data formatting | bytes 1572864
  (2 shorter events, 0.0 us)

commit v4 on v3

--- a/solution.py
+++ b/solution.py
@@ -24,9 +24,9 @@
 
 def mixer_kernel(
     hid_in, wk_in, wv_in, wq_in, wb_in, wc_in, wh_in, oc_in, oa_in,
-    lam_in, hgain_ref, cs_ref, taps_ref, ogain_ref,
+    lam_ref, hgain_ref, cs_ref, taps_ref, ogain_ref,
     out_ref,
-    hid, wp, k_own, v_own, q_src, gated, rim, u_b,
+    hid, wp, k_own, v_own, q_src, lam_in, gated, rim, u_b,
     k_all, v_all, q_own, qa, lam_own, s0, s1, s2, acc, m_ref, o_stage,
     act, wts, sbuf, rbuf, mix, stats,
     h_sem, w_sem, ow_sem, ow_send, ow_recv, rim_send, rim_recv,
@@ -68,7 +68,7 @@
             theirs = w_in.at[:, pl.ds(chunk * 1024 + (1 - c) * 512, 512)]
             own_out.append(pltpu.make_async_copy(own, dst, ow_sem.at[k]))
             pair_out.append(partner(theirs, dst, ow_send.at[k], ow_recv.at[k]))
-    for one in loads:
+    for one in loads[:4]:
         one.start()
 
     barrier = pltpu.get_barrier_semaphore()
@@ -106,7 +106,12 @@
             parts += [a * cos - b * sin, b * cos + a * sin]
         return jnp.concatenate(parts, axis=0)
 
+    for e in range(2):
+        lam_in[e] = jnp.full((8, 128), lam_ref[e], F32)
+
     loads[0].wait()
+    for one in loads[4:6]:
+        one.start()
 
     def key_rows(m, carry):
         pltpu.make_async_copy(hid_in.at[0:TQ], hid.at[m], h_sem.at[m]).wait()
@@ -117,6 +122,8 @@
         return carry
 
     lax.fori_loop(0, NT, key_rows, 0)
+    for one in loads[6:]:
+        one.start()
     pl.semaphore_wait(barrier, 37)
     for one in own_out + pair_out:
         one.start()
@@ -146,6 +153,81 @@
         @pl.when(jnp.logical_not(same))
         def _():
             action()
+
+    def k_copy(blk, sems, n, xx, cc):
+        return remote(k_all.at[blk], k_all.at[blk], sems.at[n], k_recv.at[blk], z, xx, cc)
+
+    def v_copy(blk, sems, n, xx, cc):
+        part = v_all.at[blk, pl.ds(0, 128)]
+        return remote(part, part, sems.at[n], v_recv.at[blk], z, xx, cc)
+
+    def block_of(w, u):
+        side = jnp.where(u < 2, left, right)
+        col = jnp.where(w == 0, x, jnp.where(w == 3, (x + 2) % 4, side))
+        row = jnp.where(w == 2, (u + 2) % 4, u)
+        return row * 4 + col
+
+    def k_arrived(blk):
+        k_copy(blk, dk_send, 0, x, 1 - c).wait_recv()
+
+    def v_arrived(blk):
+        v_copy(blk, dv_send, 0, x, 1 - c).wait_recv()
+
+    def arrived(blk):
+        k_arrived(blk)
+        v_arrived(blk)
+
+    def pass_right(blk, n):
+        k_copy(blk, rk_send, n, right, c).start()
+        v_copy(blk, rv_send, n, right, c).start()
+
+    def pass_left(blk, n):
+        k_copy(blk, lk_send, n, left, c).start()
+        v_copy(blk, lv_send, n, left, c).start()
+
+    def pass_partner(blk, n):
+        k_copy(blk, dk_send, n, x, 1 - c).start()
+        v_copy(blk, dv_send, n, x, 1 - c).start()
+
+    low, high = c * 4 + x, (c + 2) * 4 + x
+    near = z % 2 == c
+
+    def send_low(copy, rights, lefts, partners):
+        copy(low, rights, 0, right, c).start()
+        copy(low, lefts, 1, left, c).start()
+        copy(low, partners, 0, x, 1 - c).start()
+
+    def send_high(copy, rights, lefts, partners):
+        copy(high, lefts, 0, left, c).start()
+        copy(high, rights, 1, right, c).start()
+        copy(high, partners, 1, x, 1 - c).start()
+
+    def start_own(copy, here, rights, lefts, partners):
+        @pl.when(near)
+        def _():
+            unless(z // 2 == c, lambda: here(sp))
+
+            @pl.when(z < 2)
+            def _():
+                send_low(copy, rights, lefts, partners)
+
+            @pl.when(z >= 2)
+            def _():
+                send_high(copy, rights, lefts, partners)
+
+    def start_rest(copy, here, rights, lefts, partners):
+        @pl.when(jnp.logical_not(near & (z < 2)))
+        def _():
+            here(low)
+            send_low(copy, rights, lefts, partners)
+
+        @pl.when(jnp.logical_not(near & (z >= 2)))
+        def _():
+            here(high)
+            send_high(copy, rights, lefts, partners)
+
+    k_ring = (k_copy, k_arrived, rk_send, lk_send, dk_send)
+    v_ring = (v_copy, v_arrived, rv_send, lv_send, dv_send)
 
     for e in range(2):
         unless(kv_same(e), lambda: key_first(e).start())
@@ -173,6 +255,8 @@
         def _():
             v_all[sp, 0:128, :] = v_own[e]
 
+    start_own(*k_ring)
+
     loads[5].wait()
 
     def query_rows(m, carry):
@@ -191,6 +275,8 @@
             q_own[slot_of_sp] = q_src[e]
             lam_own[slot_of_sp] = lam_in[e]
 
+    start_own(*v_ring)
+
     for n in (6, 7, 8):
         loads[n].wait()
 
@@ -199,6 +285,7 @@
         return carry
 
     lax.fori_loop(0, NT, gated_rows, 0)
+    start_rest(*k_ring)
 
     def gate_rows(m, carry):
         u_b[m] = jnp.dot(hid[m], wp[5], preferred_element_type=F32).astype(BF16)
@@ -221,24 +308,7 @@
     lax.fori_loop(0, NB, ones, 0)
     acc[...] = jnp.zeros(acc.shape, F32)
     m_ref[...] = jnp.full(m_ref.shape, NEG_LARGE, F32)
-
-    @pl.when(sp > 0)
-    def _():
-        rim_copy.wait_recv()
-        gated[0:8, :] = rim[...]
-
-    @pl.when(sp == 0)
-    def _():
-        gated[0:8, :] = jnp.zeros((8, 256), F32)
-
-    for m in range(NT):
-        total = jnp.zeros((TQ, 256), F32)
-        for tap in range(TAPS):
-            first = 8 + m * TQ - (TAPS - 1) + tap
-            total = total + taps_ref[tap : tap + 1, :] * gated[first : first + TQ, :]
-        conv = (u_b[m].astype(F32) * total).astype(BF16)
-        act[2 * c, m * TQ : (m + 1) * TQ, :] = conv[:, 0:128]
-        act[2 * c + 1, m * TQ : (m + 1) * TQ, :] = conv[:, 128:256]
+    start_rest(*v_ring)
 
     zero = jnp.zeros((QK, TQ), BF16)
     for qb in range(2):
@@ -253,13 +323,6 @@
             qa[qb * NT + t, 0:QK, TQ : 2 * TQ] = zero
             qa[qb * NT + t, QK:128, TQ : 2 * TQ] = qt[QK:128]
 
-    conv_sends = []
-    for n in range(2):
-        piece = act.at[2 * c + n]
-        conv_sends.append(partner(piece, piece, c_send.at[n], c_recv.at[n]))
-    for one in conv_sends:
-        one.start()
-
     scores = (s0, s1, s2)
 
     def unit(qb, j, diagonal):
@@ -295,45 +358,6 @@
         consume(1)
         consume(2)
 
-    def k_copy(blk, sems, n, xx, cc):
-        return remote(k_all.at[blk], k_all.at[blk], sems.at[n], k_recv.at[blk], z, xx, cc)
-
-    def v_copy(blk, sems, n, xx, cc):
-        part = v_all.at[blk, pl.ds(0, 128)]
-        return remote(part, part, sems.at[n], v_recv.at[blk], z, xx, cc)
-
-    def block_of(w, u):
-        side = jnp.where(u < 2, left, right)
-        col = jnp.where(w == 0, x, jnp.where(w == 3, (x + 2) % 4, side))
-        row = jnp.where(w == 2, (u + 2) % 4, u)
-        return row * 4 + col
-
-    def arrived(blk):
-        k_copy(blk, dk_send, 0, x, 1 - c).wait_recv()
-        v_copy(blk, dv_send, 0, x, 1 - c).wait_recv()
-
-    def pass_right(blk, n):
-        k_copy(blk, rk_send, n, right, c).start()
-        v_copy(blk, rv_send, n, right, c).start()
-
-    def pass_left(blk, n):
-        k_copy(blk, lk_send, n, left, c).start()
-        v_copy(blk, lv_send, n, left, c).start()
-
-    def pass_partner(blk, n):
-        k_copy(blk, dk_send, n, x, 1 - c).start()
-        v_copy(blk, dv_send, n, x, 1 - c).start()
-
-    low, high = c * 4 + x, (c + 2) * 4 + x
-    unless((low == sp) & (z // 2 == c), lambda: arrived(low))
-    pass_right(low, 0)
-    unless((high == sp) & (z // 2 == c), lambda: arrived(high))
-    pass_left(high, 0)
-    pass_right(high, 1)
-    pass_left(low, 1)
-    pass_partner(low, 0)
-    pass_partner(high, 1)
-
     def exchange(w):
         from_left, from_right = block_of(w, c), block_of(w, c + 2)
         arrived(from_left)
@@ -350,37 +374,6 @@
             pass_left(from_right, 2)
 
         pass_partner(from_right, 2 * w + 1)
-
-    def step(i, carry):
-        w, k = i // 4, i % 4
-        u = jnp.where(k < 2, c + 2 * k, 1 - c + 2 * (k - 2))
-        blk = block_of(w, u)
-
-        @pl.when((k == 3) & (w < 3))
-        def _():
-            exchange(w + 1)
-
-        @pl.when(k >= 2)
-        def _():
-            arrived(blk)
-
-        def for_queries(qb, carry):
-            q_blk = jnp.where(qb == 0, own_pair, 15 - own_pair)
-
-            @pl.when(blk < q_blk)
-            def _():
-                unit(qb, blk, False)
-
-            @pl.when(blk == q_blk)
-            def _():
-                unit(qb, blk, True)
-
-            return carry
-
-        lax.fori_loop(0, 2, for_queries, 0)
-        return carry
-
-    lax.fori_loop(0, NB, step, 0)
 
     def out_same(q_blk):
         return (q_blk == sp) & (z // 2 == c)
@@ -392,7 +385,9 @@
         )
 
     q_blks = (own_pair, 15 - own_pair)
-    for qb in range(2):
+
+    def finish(qb):
+        hgain = jnp.broadcast_to(hgain_ref[...].astype(F32).reshape(1, 128), (8, 128)).T[:, 0:1]
         lam = lam_own[qb, 0:1, 0:1]
         for t in range(NT):
             at = qb * NT + t
@@ -400,13 +395,83 @@
             n2 = acc[at, 0:128, TQ : 2 * TQ] / acc[at, 128:129, TQ : 2 * TQ]
             diff = n1 - lam * n2
             mean = jnp.mean(diff * diff, axis=0, keepdims=True)
-            normed = diff * lax.rsqrt(mean + 1e-05) * hgain_ref[...]
+            normed = diff * lax.rsqrt(mean + 1e-05) * hgain
             o_stage[qb, t * TQ : (t + 1) * TQ, :] = normed.T.astype(BF16)
         unless(out_same(q_blks[qb]), lambda: out_copy(qb, q_blks[qb]).start())
 
         @pl.when(out_same(q_blks[qb]))
         def _():
             act[4 + z] = o_stage[qb]
+
+    conv_sends = []
+    for n in range(2):
+        piece = act.at[2 * c + n]
+        conv_sends.append(partner(piece, piece, c_send.at[n], c_recv.at[n]))
+
+    def convolve():
+        @pl.when(sp > 0)
+        def _():
+            rim_copy.wait_recv()
+            gated[0:8, :] = rim[...]
+
+        @pl.when(sp == 0)
+        def _():
+            gated[0:8, :] = jnp.zeros((8, 256), F32)
+
+        taps = taps_ref[...].astype(F32)
+        for m in range(NT):
+            total = jnp.zeros((TQ, 256), F32)
+            for tap in range(TAPS):
+                first = 8 + m * TQ - (TAPS - 1) + tap
+                total = total + taps[tap : tap + 1, :] * gated[first : first + TQ, :]
+            conv = (u_b[m].astype(F32) * total).astype(BF16)
+            act[2 * c, m * TQ : (m + 1) * TQ, :] = conv[:, 0:128]
+            act[2 * c + 1, m * TQ : (m + 1) * TQ, :] = conv[:, 128:256]
+        for one in conv_sends:
+            one.start()
+
+    def step(i, carry):
+        w, k = i // 4, i % 4
+        plain = jnp.where(k < 2, c + 2 * k, 1 - c + 2 * (k - 2))
+        last = jnp.where(k % 2 == 0, c, 1 - c) + 2 * (k // 2)
+        u = jnp.where(w == 3, last, plain)
+        blk = block_of(w, u)
+
+        @pl.when((k == 3) & (w < 3))
+        def _():
+            exchange(w + 1)
+
+        @pl.when(u % 2 != c)
+        def _():
+            arrived(blk)
+
+        @pl.when(i == 9)
+        def _():
+            convolve()
+
+        @pl.when(i == NB - 2)
+        def _():
+            finish(0)
+
+        def for_queries(qb, carry):
+            q_blk = jnp.where(qb == 0, own_pair, 15 - own_pair)
+
+            @pl.when(blk < q_blk)
+            def _():
+                unit(qb, blk, False)
+
+            @pl.when(blk == q_blk)
+            def _():
+                unit(qb, blk, True)
+
+            return carry
+
+        lax.fori_loop(0, 2, for_queries, 0)
+        return carry
+
+    lax.fori_loop(0, NB, step, 0)
+
+    finish(1)
 
     forwards = []
     for e in range(2):
@@ -468,10 +533,11 @@
     for n in range(1, 8):
         everything = everything + stats[n]
     columns = everything.T
+    ogain = ogain_ref[pl.ds(pl.multiple_of(tp * 512, 512), 512)].astype(F32).reshape(1, 512)
     mean = columns[:, 0:1] * (1.0 / D)
     variance = columns[:, 1:2] * (1.0 / D) - mean * mean
     out_ref[...] = (
-        (mix[...].astype(F32) - mean) * lax.rsqrt(variance + 1e-05) * ogain_ref[tp]
+        (mix[...].astype(F32) - mean) * lax.rsqrt(variance + 1e-05) * ogain
     ).astype(BF16)
 
 
@@ -511,7 +577,7 @@
     return pl.pallas_call(
         mixer_kernel,
         out_shape=jax.ShapeDtypeStruct((TB, 512), BF16),
-        in_specs=[hbm] * 9 + [vmem] * 5,
+        in_specs=[hbm] * 9 + [pl.BlockSpec(memory_space=pltpu.SMEM)] + [vmem] * 4,
         out_specs=vmem,
         scratch_shapes=[
             pltpu.VMEM((NT, TQ, D), BF16),
@@ -519,6 +585,7 @@
             pltpu.VMEM((2, TB, 128), BF16),
             pltpu.VMEM((2, 128, TB), BF16),
             pltpu.VMEM((2, 128, TB), BF16),
+            pltpu.VMEM((2, 8, 128), F32),
             pltpu.VMEM((TB + 8, 256), F32),
             pltpu.VMEM((8, 256), F32),
             pltpu.VMEM((NT, TQ, 256), BF16),
@@ -577,11 +644,11 @@
     return mixer(
         hidden_states, w_key, w_value, w_query, w_conv_b, w_conv_c, w_conv_h,
         w_out_conv, w_out_attn,
-        jnp.broadcast_to(lambdas[:, None, None], (2, 8, 128)),
-        head_gain.astype(F32)[:, None],
+        lambdas,
+        head_gain,
         table,
-        conv_taps.astype(F32),
-        out_gain.astype(F32).reshape(8, 1, 512),
+        conv_taps,
+        out_gain,
     )
 
 

time: 117 us -> 109 us (0.932)
  other arithmetic: 4.36 us -> 1.13 us
  local copies, waits for them, and re-layouts: 4.12 us -> 2.06 us
  Pallas kernels: 107 us -> 105 us
    broadcast_in_dim x2 -> x0, local copies, waits for them, and re-layouts: 2.06 us -> none  [the longest x1 1.32 us: per_device(): jnp.broadcast_to(lambdas[:, None, None], (2, 8, 128))]
    pallas_call x1, Pallas kernels: 107 us -> 105 us  [mixer(): pl.pallas_call(mixer_kernel, out_shape=jax.ShapeDtypeStruct((TB, 512), BF...]
    reshape x1 -> x0, other arithmetic: 1.29 us -> none  [per_device(): out_gain.astype(F32).reshape(8, 1, 512)]
    convert_element_type x1 -> x0, other arithmetic: 1.28 us -> none  [per_device(): conv_taps.astype(F32)]
where the time goes in v4:
time: 109 us; the launch traced here: 108 us
  Pallas kernels  105 us (96%)
  local copies, waits for them, and re-layouts  2.06 us (2%)
  other arithmetic  1.13 us (1%)
    pallas_call x1, Pallas kernels, mixer(): pl.pallas_call(mixer_kernel, out_shape=jax.ShapeDtypeStruct((TB, 512), BF...  105 us

profile of v4, /device:TPU:1, one launch (start us, length us, event | category | flops | bytes accessed | tf_op | source)
XLA Modules:
  0.0 108.4 jit_solution(4361679790533436162)
XLA Ops:
  0.0 0.4 multiply_cosine_fusion
  0.4 0.7 pad_maximum_fusion.cs_ref
  1.1 105.2 %mixer.1 = bf16[768,512]{1,0:T(8,128)(2,1)} custom-call(bf16[768,4096]{1,0:T(8,128)(2,1)} %hid_in.1, bf16[4096,256]{1,0:T(8,128)(2,1)} %wk_in.1, bf16[4096,256]{1,0:T(8,128)(2,1)} %wv_in.1, bf16[4096,256]{1,0:T(8,128)(2,1)} %wq_in.1, bf16[4096,256]{1,0:T(8,128)(2,1)} %wb_in.1, bf16[4096,256]{1,0:T(8,128)(2,1)} %wc_in.1, bf16[4096,256]{1,0:T(8,128)(2,1)} %wh_in.1, ...), custom_call_target="tpu_custom_call" | custom-call | tf_op jit(solution)/shard_map/mixer/pallas_call | solution.py:577
  106.4 2.1 %copy.15 = bf16[768,512]{1,0:T(8,128)(2,1)} copy(bf16[768,512]{1,0:T(8,128)(2,1)} %mixer.1) | data formatting | bytes 1572864
  (2 shorter events, 0.0 us)

commit v5 on v4

--- a/solution.py
+++ b/solution.py
@@ -13,9 +13,8 @@
 TQ = 256
 NT = TB // TQ
 VA = 144
-SUB = 2
 HALF = TB // 2
-PR = HALF // SUB
+PR = HALF // 2
 LOG2E = 1.4426950408889634
 NEG_LARGE = -1e30
 BF16 = jnp.bfloat16
@@ -26,20 +25,20 @@
     hid_in, wk_in, wv_in, wq_in, wb_in, wc_in, wh_in, oc_in, oa_in,
     lam_ref, hgain_ref, cs_ref, taps_ref, ogain_ref,
     out_ref,
-    hid, wp, k_own, v_own, q_src, lam_in, gated, rim, u_b,
+    hid, wp, k_own, v_own, q_src, lam_in, gated, halo, u_b,
     k_all, v_all, q_own, qa, lam_own, s0, s1, s2, acc, m_ref, o_stage,
-    act, wts, sbuf, rbuf, mix, stats,
-    h_sem, w_sem, ow_sem, ow_send, ow_recv, rim_send, rim_recv,
+    act, wtc, wta, sbuf, rbuf, mixc, mix, stats,
+    h_sem, w_sem, ow_sem, ow_send, ow_recv, aw_sem, aw_send, aw_recv, halo_send, halo_recv,
     k_recv, v_recv, q_recv, l_recv, o_recv,
     q_send, l_send, p1k_send, p1v_send, rk_send, rv_send, lk_send, lv_send,
     dk_send, dv_send, o_send,
-    c_send, c_recv, f_send, f_recv, r_send, r_recv, t_send, t_recv,
+    c_send, c_recv, f_send, r_send, r_recv, t_send, t_recv,
 ):
     sp = lax.axis_index("sp")
     tp = lax.axis_index("tp")
     z, x = sp // 4, sp % 4
     y, c = tp // 2, tp % 2
-    own_pair = x + 4 * c
+    own_pair = jnp.where(z < 2, x, 3 - x) + 4 * c
     left, right = (x + 3) % 4, (x + 1) % 4
 
     def copy_to(src, dst, send_sem, recv_sem, at_sp, at_tp):
@@ -61,13 +60,20 @@
         loads.append(pltpu.make_async_copy(w_in, wp.at[n + 1], w_sem.at[n + 1]))
     own_out, pair_out = [], []
     for chunk in range(4):
-        for n, w_in in enumerate((oc_in, oa_in)):
-            dst = wts.at[chunk, pl.ds(n * 512 + c * 256, 256)]
-            k = chunk * 2 + n
-            own = w_in.at[:, pl.ds(chunk * 1024 + c * 512, 512)]
-            theirs = w_in.at[:, pl.ds(chunk * 1024 + (1 - c) * 512, 512)]
-            own_out.append(pltpu.make_async_copy(own, dst, ow_sem.at[k]))
-            pair_out.append(partner(theirs, dst, ow_send.at[k], ow_recv.at[k]))
+        dst = wtc.at[chunk, pl.ds(c * 256, 256)]
+        own = oc_in.at[:, pl.ds(chunk * 1024 + c * 512, 512)]
+        theirs = oc_in.at[:, pl.ds(chunk * 1024 + (1 - c) * 512, 512)]
+        own_out.append(pltpu.make_async_copy(own, dst, ow_sem.at[chunk]))
+        pair_out.append(partner(theirs, dst, ow_send.at[chunk], ow_recv.at[chunk]))
+    own_out.append(pltpu.make_async_copy(oa_in.at[:, pl.ds(tp * 512, 512)], wta.at[tp], aw_sem))
+    for i in range(1, 8):
+        other = (tp + i) % 8
+        pair_out.append(copy_to(
+            oa_in.at[:, pl.ds(other * 512, 512)], wta.at[tp], aw_send.at[i - 1], aw_recv.at[i - 1], sp, other
+        ))
+    halo_copy = copy_to(
+        hid_in.at[pl.ds(TB - 16, 16)], halo, halo_send, halo_recv, (sp + 1) % 16, tp
+    )
     for one in loads[:4]:
         one.start()
 
@@ -89,6 +95,21 @@
         )
         return carry
 
+    pair_of_sp = jnp.where(sp < 8, sp, 15 - sp)
+    slot_of_sp = jnp.where(sp < 8, 0, 1)
+    pair_col = jnp.where(c == 0, pair_of_sp % 4, 3 - pair_of_sp % 4)
+    q_blks = (own_pair, 15 - own_pair)
+    for up in range(1, 4):
+        plane = ((y + up) % 4) * 2
+        for e in range(2):
+            for at_sp, at_tp in (
+                (q_blks[e], plane + z // 2),
+                ((2 * c + e) * 4 + pair_col, plane + pair_of_sp // 4),
+            ):
+                pl.semaphore_signal(
+                    barrier, inc=1, device_id={"sp": at_sp, "tp": at_tp},
+                    device_id_type=pl.DeviceIdType.MESH,
+                )
     lax.fori_loop(1, 32, greet_plane, 0)
     lax.fori_loop(0, 6, greet_column, 0)
 
@@ -124,18 +145,18 @@
     lax.fori_loop(0, NT, key_rows, 0)
     for one in loads[6:]:
         one.start()
-    pl.semaphore_wait(barrier, 37)
-    for one in own_out + pair_out:
-        one.start()
-
-    pair_of_sp = jnp.where(sp < 8, sp, 15 - sp)
-    slot_of_sp = jnp.where(sp < 8, 0, 1)
+    pl.semaphore_wait(barrier, 49)
+
+    @pl.when(sp < 15)
+    def _():
+        halo_copy.start()
+
 
     def kv_same(e):
         return (2 * c + e == z) & (z % 2 == c)
 
     def q_same(e):
-        return (2 * c + e == z) & (pair_of_sp % 4 == x) & (pair_of_sp // 4 == c)
+        return (2 * c + e == z) & (pair_col == x) & (pair_of_sp // 4 == c)
 
     def key_first(e):
         return remote(k_own.at[e], k_all.at[sp], p1k_send.at[e], k_recv.at[sp], 2 * c + e, x, z % 2)
@@ -144,10 +165,10 @@
         return remote(v_own.at[e], v_all.at[sp, pl.ds(0, 128)], p1v_send.at[e], v_recv.at[sp], 2 * c + e, x, z % 2)
 
     def query_first(e):
-        return remote(q_src.at[e], q_own.at[slot_of_sp], q_send.at[e], q_recv.at[slot_of_sp], 2 * c + e, pair_of_sp % 4, pair_of_sp // 4)
+        return remote(q_src.at[e], q_own.at[slot_of_sp], q_send.at[e], q_recv.at[slot_of_sp], 2 * c + e, pair_col, pair_of_sp // 4)
 
     def lam_first(e):
-        return remote(lam_in.at[e], lam_own.at[slot_of_sp], l_send.at[e], l_recv.at[slot_of_sp], 2 * c + e, pair_of_sp % 4, pair_of_sp // 4)
+        return remote(lam_in.at[e], lam_own.at[slot_of_sp], l_send.at[e], l_recv.at[slot_of_sp], 2 * c + e, pair_col, pair_of_sp // 4)
 
     def unless(same, action):
         @pl.when(jnp.logical_not(same))
@@ -236,6 +257,9 @@
         def _():
             k_all[sp] = k_own[e]
 
+    for one in own_out + pair_out:
+        one.start()
+
     def column(m):
         return pl.ds(pl.multiple_of(m * TQ, TQ), TQ)
 
@@ -277,29 +301,28 @@
 
     start_own(*v_ring)
 
-    for n in (6, 7, 8):
-        loads[n].wait()
+    loads[6].wait()
 
     def gated_rows(m, carry):
-        gated[pl.ds(pl.multiple_of(8 + m * TQ, 8), TQ), :] = project(m, 3) * project(m, 4)
-        return carry
-
+        rows = pl.ds(pl.multiple_of(8 + m * TQ, 8), TQ)
+        gated[rows, :] = gated[rows, :] * project(m, 4)
+        return carry
+
+    def inner_rows(m, carry):
+        gated[pl.ds(pl.multiple_of(8 + m * TQ, 8), TQ), :] = project(m, 3)
+        return carry
+
+    lax.fori_loop(0, NT, inner_rows, 0)
+    start_rest(*k_ring)
+    loads[7].wait()
     lax.fori_loop(0, NT, gated_rows, 0)
-    start_rest(*k_ring)
+    loads[8].wait()
 
     def gate_rows(m, carry):
         u_b[m] = jnp.dot(hid[m], wp[5], preferred_element_type=F32).astype(BF16)
         return carry
 
     lax.fori_loop(0, NT, gate_rows, 0)
-
-    rim_copy = copy_to(
-        gated.at[pl.ds(TB, 8)], rim, rim_send, rim_recv, (sp + 1) % 16, tp
-    )
-
-    @pl.when(sp < 15)
-    def _():
-        rim_copy.start()
 
     def ones(j, carry):
         v_all[j, 128:VA, :] = jnp.ones((VA - 128, TB), BF16)
@@ -378,13 +401,13 @@
     def out_same(q_blk):
         return (q_blk == sp) & (z // 2 == c)
 
-    def out_copy(qb, q_blk):
-        return remote(
-            o_stage.at[qb], act.at[4 + z], o_send.at[qb], o_recv.at[z % 2],
-            q_blk // 4, q_blk % 4, z // 2,
-        )
-
-    q_blks = (own_pair, 15 - own_pair)
+    def out_copies(qb):
+        for n in range(4):
+            plane = (y + n) % 4
+            yield n, copy_to(
+                o_stage.at[qb], act.at[4 + y * 4 + z], o_send.at[qb, n], o_recv.at[y * 4 + z],
+                q_blks[qb], plane * 2 + z // 2,
+            )
 
     def finish(qb):
         hgain = jnp.broadcast_to(hgain_ref[...].astype(F32).reshape(1, 128), (8, 128)).T[:, 0:1]
@@ -397,11 +420,15 @@
             mean = jnp.mean(diff * diff, axis=0, keepdims=True)
             normed = diff * lax.rsqrt(mean + 1e-05) * hgain
             o_stage[qb, t * TQ : (t + 1) * TQ, :] = normed.T.astype(BF16)
-        unless(out_same(q_blks[qb]), lambda: out_copy(qb, q_blks[qb]).start())
+        for n, one in out_copies(qb):
+            if n == 0:
+                unless(out_same(q_blks[qb]), lambda: one.start())
+            else:
+                one.start()
 
         @pl.when(out_same(q_blks[qb]))
         def _():
-            act[4 + z] = o_stage[qb]
+            act[4 + y * 4 + z] = o_stage[qb]
 
     conv_sends = []
     for n in range(2):
@@ -411,8 +438,10 @@
     def convolve():
         @pl.when(sp > 0)
         def _():
-            rim_copy.wait_recv()
-            gated[0:8, :] = rim[...]
+            halo_copy.wait_recv()
+            inner = jnp.dot(halo[...], wp[3], preferred_element_type=F32).astype(BF16)
+            outer = jnp.dot(halo[...], wp[4], preferred_element_type=F32).astype(BF16)
+            gated[0:8, :] = inner[8:16].astype(F32) * outer[8:16].astype(F32)
 
         @pl.when(sp == 0)
         def _():
@@ -430,6 +459,31 @@
         for one in conv_sends:
             one.start()
 
+    convolve()
+
+    up, down = ((y + 1) % 4) * 2 + c, ((y + 3) % 4) * 2 + c
+
+    def ring(s, d):
+        return copy_to(
+            sbuf.at[s, d], rbuf.at[s, d], r_send.at[s, d], r_recv.at[s, d],
+            sp, up if d == 0 else down,
+        )
+
+    def conv_ring(s):
+        for d in range(2):
+            chunk = (y + 3 - s) % 4 if d == 0 else (y + 1 + s) % 4
+            first = d * HALF
+            rows = jnp.concatenate([act[n, first : first + HALF, :] for n in range(4)], axis=1)
+            part = jnp.dot(rows, wtc[chunk], preferred_element_type=F32)
+            if s > 0:
+                ring(s - 1, d).wait_recv()
+                part = part + rbuf[s - 1, d].astype(F32)
+            if s < 3:
+                sbuf[s, d] = part.astype(BF16)
+                ring(s, d).start()
+            else:
+                mixc[first : first + HALF, :] = part
+
     def step(i, carry):
         w, k = i // 4, i % 4
         plain = jnp.where(k < 2, c + 2 * k, 1 - c + 2 * (k - 2))
@@ -445,9 +499,16 @@
         def _():
             arrived(blk)
 
-        @pl.when(i == 9)
-        def _():
-            convolve()
+        for s, when in enumerate((2, 8, 14)):
+
+            @pl.when(i == when)
+            def _():
+                if s == 0:
+                    for one in own_out:
+                        one.wait()
+                    for one in pair_out[:4] + conv_sends:
+                        one.wait_recv()
+                conv_ring(s)
 
         @pl.when(i == NB - 2)
         def _():
@@ -473,42 +534,35 @@
 
     finish(1)
 
+    conv_ring(3)
+
+    def piece(head):
+        return act.at[4 + head]
+
+    def o_arrived(head):
+        partner(piece(head), piece(head), f_send.at[0], o_recv.at[head]).wait_recv()
+
     forwards = []
-    for e in range(2):
-        head = 2 * c + e
-        made_here = (head == z) & ((sp == own_pair) | (sp == 15 - own_pair))
-        piece = act.at[4 + head]
-        unless(made_here, lambda: remote(o_stage.at[0], piece, o_send.at[0], o_recv.at[e], z, x, 1 - c).wait_recv())
-        forwards.append(partner(piece, piece, f_send.at[e], f_recv.at[e]))
-        forwards[e].start()
-    for one in own_out:
-        one.wait()
-    for one in pair_out + conv_sends + forwards:
+    for n in (0, 1, 3, 2):
+        for e in range(2):
+            head = ((y + n) % 4) * 4 + 2 * c + e
+            if n == 0:
+                made_here = (2 * c + e == z) & ((sp == own_pair) | (sp == 15 - own_pair))
+                unless(made_here, lambda: o_arrived(head))
+            else:
+                o_arrived(head)
+            forwards.append(partner(piece(head), piece(head), f_send.at[len(forwards)], o_recv.at[head]))
+            forwards[-1].start()
+    for one in pair_out[4:]:
         one.wait_recv()
-
-    up, down = ((y + 1) % 4) * 2 + c, ((y + 3) % 4) * 2 + c
-
-    def ring(s, d, u):
-        return copy_to(
-            sbuf.at[s, d, u], rbuf.at[s, d, u], r_send.at[s, d, u], r_recv.at[s, d, u],
-            sp, up if d == 0 else down,
-        )
-
-    for s in range(4):
-        for u in range(SUB):
-            for d in range(2):
-                chunk = (y + 3 - s) % 4 if d == 0 else (y + 1 + s) % 4
-                first = d * HALF + u * PR
-                rows = jnp.concatenate([act[n, first : first + PR, :] for n in range(8)], axis=1)
-                part = jnp.dot(rows, wts[chunk], preferred_element_type=F32)
-                if s > 0:
-                    ring(s - 1, d, u).wait_recv()
-                    part = part + rbuf[s - 1, d, u].astype(F32)
-                if s < 3:
-                    sbuf[s, d, u] = part.astype(BF16)
-                    ring(s, d, u).start()
-                else:
-                    mix[first : first + PR, :] = part.astype(BF16)
+    for n in (0, 1, 3, 2):
+        for e in range(2):
+            o_arrived(((y + n) % 4) * 4 + 2 * (1 - c) + e)
+    for n in range(4):
+        first = n * PR
+        rows = jnp.concatenate([act[4 + h, first : first + PR, :] for h in range(16)], axis=1)
+        part = jnp.dot(rows, wta[...].reshape(2048, 512), preferred_element_type=F32)
+        mix[first : first + PR, :] = (part + mixc[first : first + PR, :]).astype(BF16)
 
     ones_row = jnp.ones((8, 512), BF16)
     dims = (((1,), (1,)), ((), ()))
@@ -546,11 +600,15 @@
         unless(kv_same(e), lambda: value_first(e).wait_send())
         unless(q_same(e), lambda: query_first(e).wait_send())
         unless(q_same(e), lambda: lam_first(e).wait_send())
-        unless(out_same(q_blks[e]), lambda: out_copy(e, q_blks[e]).wait_send())
+        for n, one in out_copies(e):
+            if n == 0:
+                unless(out_same(q_blks[e]), lambda: one.wait_send())
+            else:
+                one.wait_send()
 
     @pl.when(sp < 15)
     def _():
-        rim_copy.wait_send()
+        halo_copy.wait_send()
 
     for n in range(3):
         k_copy(0, rk_send, n, right, c).wait_send()
@@ -564,8 +622,7 @@
         one.wait_send()
     for s in range(3):
         for d in range(2):
-            for u in range(SUB):
-                ring(s, d, u).wait_send()
+            ring(s, d).wait_send()
     for i in range(1, 8):
         tell(i).wait_send()
 
@@ -587,7 +644,7 @@
             pltpu.VMEM((2, 128, TB), BF16),
             pltpu.VMEM((2, 8, 128), F32),
             pltpu.VMEM((TB + 8, 256), F32),
-            pltpu.VMEM((8, 256), F32),
+            pltpu.VMEM((16, D), BF16),
             pltpu.VMEM((NT, TQ, 256), BF16),
             pltpu.VMEM((NB, TB, 128), BF16),
             pltpu.VMEM((NB, VA, TB), BF16),
@@ -600,19 +657,21 @@
             pltpu.VMEM((2 * NT, VA, 2 * TQ), F32),
             pltpu.VMEM((2 * NT, 1, 2 * TQ), F32),
             pltpu.VMEM((2, TB, 128), BF16),
-            pltpu.VMEM((8, TB, 128), BF16),
-            pltpu.VMEM((4, 1024, 512), BF16),
-            pltpu.VMEM((3, 2, SUB, PR, 512), BF16),
-            pltpu.VMEM((3, 2, SUB, PR, 512), BF16),
+            pltpu.VMEM((20, TB, 128), BF16),
+            pltpu.VMEM((4, 512, 512), BF16),
+            pltpu.VMEM((8, 256, 512), BF16),
+            pltpu.VMEM((3, 2, HALF, 512), BF16),
+            pltpu.VMEM((3, 2, HALF, 512), BF16),
+            pltpu.VMEM((TB, 512), F32),
             pltpu.VMEM((TB, 512), BF16),
             pltpu.VMEM((8, 8, TB), F32),
-            dma((NT,)), dma((6,)), dma((8,)), dma((8,)), dma((8,)), dma, dma,
-            dma((NB,)), dma((NB,)), dma((2,)), dma((2,)), dma((2,)),
+            dma((NT,)), dma((6,)), dma((4,)), dma((4,)), dma((4,)), dma, dma((7,)), dma((7,)), dma, dma,
+            dma((NB,)), dma((NB,)), dma((2,)), dma((2,)), dma((16,)),
             dma((2,)), dma((2,)), dma((2,)), dma((2,)),
             dma((3,)), dma((3,)), dma((3,)), dma((3,)),
-            dma((8,)), dma((8,)), dma((2,)),
-            dma((2,)), dma((2,)), dma((2,)), dma((2,)),
-            dma((3, 2, SUB)), dma((3, 2, SUB)), dma((7,)), dma((7,)),
+            dma((8,)), dma((8,)), dma((2, 4)),
+            dma((2,)), dma((2,)), dma((8,)),
+            dma((3, 2)), dma((3, 2)), dma((7,)), dma((7,)),
         ],
         compiler_params=pltpu.CompilerParams(
             collective_id=0, has_side_effects=True, vmem_limit_bytes=67043328

time: 109 us -> 99.9 us (0.917)
  Pallas kernels: 105 us -> 96.3 us
    pallas_call x1, Pallas kernels: 105 us -> 96.3 us  [mixer(): pl.pallas_call(mixer_kernel, out_shape=jax.ShapeDtypeStruct((TB, 512), BF...]
where the time goes in v5:
time: 99.9 us; the launch traced here: 99.5 us
  Pallas kernels  96.3 us (96%)
  local copies, waits for them, and re-layouts  2.06 us (2%)
  other arithmetic  1.13 us (1%)
    pallas_call x1, Pallas kernels, mixer(): pl.pallas_call(mixer_kernel, out_shape=jax.ShapeDtypeStruct((TB, 512), BF...  96.3 us
    unnamed x1, local copies, waits for them, and re-layouts  2.06 us

profile of v5, /device:TPU:1, one launch (start us, length us, event | category | flops | bytes accessed | tf_op | source)
XLA Modules:
  0.0 99.5 jit_solution(13395720305350653331)
XLA Ops:
  0.0 0.4 multiply_cosine_fusion
  0.4 0.7 pad_maximum_fusion.cs_ref
  1.1 96.3 %mixer.1 = bf16[768,512]{1,0:T(8,128)(2,1)} custom-call(bf16[768,4096]{1,0:T(8,128)(2,1)} %hid_in.1, bf16[4096,256]{1,0:T(8,128)(2,1)} %wk_in.1, bf16[4096,256]{1,0:T(8,128)(2,1)} %wv_in.1, bf16[4096,256]{1,0:T(8,128)(2,1)} %wq_in.1, bf16[4096,256]{1,0:T(8,128)(2,1)} %wb_in.1, bf16[4096,256]{1,0:T(8,128)(2,1)} %wc_in.1, bf16[4096,256]{1,0:T(8,128)(2,1)} %wh_in.1, ...), custom_call_target="tpu_custom_call" | custom-call | tf_op jit(solution)/shard_map/mixer/pallas_call | solution.py:634
  97.5 2.1 %copy.15 = bf16[768,512]{1,0:T(8,128)(2,1)} copy(bf16[768,512]{1,0:T(8,128)(2,1)} %mixer.1) | data formatting | bytes 1572864
  (2 shorter events, 0.0 us)

commit v6 on v5

--- a/solution.py
+++ b/solution.py
@@ -28,7 +28,7 @@
     hid, wp, k_own, v_own, q_src, lam_in, gated, halo, u_b,
     k_all, v_all, q_own, qa, lam_own, s0, s1, s2, acc, m_ref, o_stage,
     act, wtc, wta, sbuf, rbuf, mixc, mix, stats,
-    h_sem, w_sem, ow_sem, ow_send, ow_recv, aw_sem, aw_send, aw_recv, halo_send, halo_recv,
+    h_sem, w_sem, ow_sem, ow_send, ow_recv, aw_sem, aw_send, aw_recv, zw_send, zw_recv, halo_send, halo_recv,
     k_recv, v_recv, q_recv, l_recv, o_recv,
     q_send, l_send, p1k_send, p1v_send, rk_send, rv_send, lk_send, lv_send,
     dk_send, dv_send, o_send,
@@ -66,11 +66,16 @@
         own_out.append(pltpu.make_async_copy(own, dst, ow_sem.at[chunk]))
         pair_out.append(partner(theirs, dst, ow_send.at[chunk], ow_recv.at[chunk]))
     own_out.append(pltpu.make_async_copy(oa_in.at[:, pl.ds(tp * 512, 512)], wta.at[tp], aw_sem))
+    half = pl.ds((z % 2) * 128, 128)
+    near_z = z + 1 - 2 * (z % 2)
+    zcopies = []
     for i in range(1, 8):
         other = (tp + i) % 8
         pair_out.append(copy_to(
-            oa_in.at[:, pl.ds(other * 512, 512)], wta.at[tp], aw_send.at[i - 1], aw_recv.at[i - 1], sp, other
+            oa_in.at[half, pl.ds(other * 512, 512)], wta.at[tp, half], aw_send.at[i - 1], aw_recv.at[i - 1], sp, other
         ))
+        piece_of = wta.at[(tp + 8 - i) % 8, half]
+        zcopies.append(remote(piece_of, piece_of, zw_send.at[i - 1], zw_recv.at[i - 1], near_z, x, c))
     halo_copy = copy_to(
         hid_in.at[pl.ds(TB - 16, 16)], halo, halo_send, halo_recv, (sp + 1) % 16, tp
     )
@@ -99,17 +104,6 @@
     slot_of_sp = jnp.where(sp < 8, 0, 1)
     pair_col = jnp.where(c == 0, pair_of_sp % 4, 3 - pair_of_sp % 4)
     q_blks = (own_pair, 15 - own_pair)
-    for up in range(1, 4):
-        plane = ((y + up) % 4) * 2
-        for e in range(2):
-            for at_sp, at_tp in (
-                (q_blks[e], plane + z // 2),
-                ((2 * c + e) * 4 + pair_col, plane + pair_of_sp // 4),
-            ):
-                pl.semaphore_signal(
-                    barrier, inc=1, device_id={"sp": at_sp, "tp": at_tp},
-                    device_id_type=pl.DeviceIdType.MESH,
-                )
     lax.fori_loop(1, 32, greet_plane, 0)
     lax.fori_loop(0, 6, greet_column, 0)
 
@@ -145,7 +139,7 @@
     lax.fori_loop(0, NT, key_rows, 0)
     for one in loads[6:]:
         one.start()
-    pl.semaphore_wait(barrier, 49)
+    pl.semaphore_wait(barrier, 37)
 
     @pl.when(sp < 15)
     def _():
@@ -401,13 +395,11 @@
     def out_same(q_blk):
         return (q_blk == sp) & (z // 2 == c)
 
-    def out_copies(qb):
-        for n in range(4):
-            plane = (y + n) % 4
-            yield n, copy_to(
-                o_stage.at[qb], act.at[4 + y * 4 + z], o_send.at[qb, n], o_recv.at[y * 4 + z],
-                q_blks[qb], plane * 2 + z // 2,
-            )
+    def out_copy(qb):
+        return remote(
+            o_stage.at[qb], act.at[4 + y * 4 + z], o_send.at[qb], o_recv.at[y * 4 + z],
+            q_blks[qb] // 4, q_blks[qb] % 4, z // 2,
+        )
 
     def finish(qb):
         hgain = jnp.broadcast_to(hgain_ref[...].astype(F32).reshape(1, 128), (8, 128)).T[:, 0:1]
@@ -420,11 +412,7 @@
             mean = jnp.mean(diff * diff, axis=0, keepdims=True)
             normed = diff * lax.rsqrt(mean + 1e-05) * hgain
             o_stage[qb, t * TQ : (t + 1) * TQ, :] = normed.T.astype(BF16)
-        for n, one in out_copies(qb):
-            if n == 0:
-                unless(out_same(q_blks[qb]), lambda: one.start())
-            else:
-                one.start()
+        unless(out_same(q_blks[qb]), lambda: out_copy(qb).start())
 
         @pl.when(out_same(q_blks[qb]))
         def _():
@@ -499,7 +487,13 @@
         def _():
             arrived(blk)
 
-        for s, when in enumerate((2, 8, 14)):
+        @pl.when(i == 3)
+        def _():
+            for n in range(7):
+                pair_out[4 + n].wait_recv()
+                zcopies[n].start()
+
+        for s, when in enumerate((1, 7, 12)):
 
             @pl.when(i == when)
             def _():
@@ -543,17 +537,36 @@
         partner(piece(head), piece(head), f_send.at[0], o_recv.at[head]).wait_recv()
 
     forwards = []
-    for n in (0, 1, 3, 2):
-        for e in range(2):
-            head = ((y + n) % 4) * 4 + 2 * c + e
-            if n == 0:
-                made_here = (2 * c + e == z) & ((sp == own_pair) | (sp == 15 - own_pair))
-                unless(made_here, lambda: o_arrived(head))
-            else:
-                o_arrived(head)
-            forwards.append(partner(piece(head), piece(head), f_send.at[len(forwards)], o_recv.at[head]))
-            forwards[-1].start()
-    for one in pair_out[4:]:
+
+    def pass_on(head, target):
+        one = copy_to(piece(head), piece(head), f_send.at[len(forwards)], o_recv.at[head], sp, target)
+        one.start()
+        forwards.append(one)
+
+    beside = y * 2 + (1 - c)
+    mine = [y * 4 + 2 * c + e for e in range(2)]
+    below = [((y + 3) % 4) * 4 + 2 * c + e for e in range(2)]
+    above = [((y + 1) % 4) * 4 + 2 * c + e for e in range(2)]
+    across = [((y + 2) % 4) * 4 + 2 * c + e for e in range(2)]
+    here = (sp == own_pair) | (sp == 15 - own_pair)
+    unless((2 * c == z) & here, lambda: o_arrived(mine[0]))
+    pass_on(mine[0], up)
+    unless((2 * c + 1 == z) & here, lambda: o_arrived(mine[1]))
+    pass_on(mine[1], down)
+    pass_on(mine[1], up)
+    pass_on(mine[0], down)
+    pass_on(mine[0], beside)
+    pass_on(mine[1], beside)
+    o_arrived(below[0])
+    pass_on(below[0], up)
+    o_arrived(above[1])
+    pass_on(above[1], down)
+    pass_on(below[0], beside)
+    pass_on(above[1], beside)
+    for head in (below[1], above[0], across[0], across[1]):
+        o_arrived(head)
+        pass_on(head, beside)
+    for one in zcopies:
         one.wait_recv()
     for n in (0, 1, 3, 2):
         for e in range(2):
@@ -600,11 +613,7 @@
         unless(kv_same(e), lambda: value_first(e).wait_send())
         unless(q_same(e), lambda: query_first(e).wait_send())
         unless(q_same(e), lambda: lam_first(e).wait_send())
-        for n, one in out_copies(e):
-            if n == 0:
-                unless(out_same(q_blks[e]), lambda: one.wait_send())
-            else:
-                one.wait_send()
+        unless(out_same(q_blks[e]), lambda: out_copy(e).wait_send())
 
     @pl.when(sp < 15)
     def _():
@@ -618,7 +627,7 @@
     for n in range(8):
         k_copy(0, dk_send, n, x, 1 - c).wait_send()
         v_copy(0, dv_send, n, x, 1 - c).wait_send()
-    for one in pair_out + conv_sends + forwards:
+    for one in pair_out + zcopies + conv_sends + forwards:
         one.wait_send()
     for s in range(3):
         for d in range(2):
@@ -665,12 +674,12 @@
             pltpu.VMEM((TB, 512), F32),
             pltpu.VMEM((TB, 512), BF16),
             pltpu.VMEM((8, 8, TB), F32),
-            dma((NT,)), dma((6,)), dma((4,)), dma((4,)), dma((4,)), dma, dma((7,)), dma((7,)), dma, dma,
+            dma((NT,)), dma((6,)), dma((4,)), dma((4,)), dma((4,)), dma, dma((7,)), dma((7,)), dma((7,)), dma((7,)), dma, dma,
             dma((NB,)), dma((NB,)), dma((2,)), dma((2,)), dma((16,)),
             dma((2,)), dma((2,)), dma((2,)), dma((2,)),
             dma((3,)), dma((3,)), dma((3,)), dma((3,)),
-            dma((8,)), dma((8,)), dma((2, 4)),
-            dma((2,)), dma((2,)), dma((8,)),
+            dma((8,)), dma((8,)), dma((2,)),
+            dma((2,)), dma((2,)), dma((14,)),
             dma((3, 2)), dma((3, 2)), dma((7,)), dma((7,)),
         ],
         compiler_params=pltpu.CompilerParams(

time: 99.9 us -> 94.9 us (0.950)
  Pallas kernels: 96.3 us -> 90.4 us
    pallas_call x1, Pallas kernels: 96.3 us -> 90.4 us  [mixer(): pl.pallas_call(mixer_kernel, out_shape=jax.ShapeDtypeStruct((TB, 512), BF...]
where the time goes in v6:
time: 94.9 us; the launch traced here: 93.7 us
  Pallas kernels  90.4 us (95%)
  local copies, waits for them, and re-layouts  2.06 us (2%)
  other arithmetic  1.13 us (1%)
    pallas_call x1, Pallas kernels, mixer(): pl.pallas_call(mixer_kernel, out_shape=jax.ShapeDtypeStruct((TB, 512), BF...  90.4 us
    unnamed x1, local copies, waits for them, and re-layouts  2.06 us

profile of v6, /device:TPU:1, one launch (start us, length us, event | category | flops | bytes accessed | tf_op | source)
XLA Modules:
  0.0 93.7 jit_solution(10606936498336188157)
XLA Ops:
  0.0 0.4 multiply_cosine_fusion
  0.4 0.7 pad_maximum_fusion.cs_ref
  1.1 90.4 %mixer.1 = bf16[768,512]{1,0:T(8,128)(2,1)} custom-call(bf16[768,4096]{1,0:T(8,128)(2,1)} %hid_in.1, bf16[4096,256]{1,0:T(8,128)(2,1)} %wk_in.1, bf16[4096,256]{1,0:T(8,128)(2,1)} %wv_in.1, bf16[4096,256]{1,0:T(8,128)(2,1)} %wq_in.1, bf16[4096,256]{1,0:T(8,128)(2,1)} %wb_in.1, bf16[4096,256]{1,0:T(8,128)(2,1)} %wc_in.1, bf16[4096,256]{1,0:T(8,128)(2,1)} %wh_in.1, ...), custom_call_target="tpu_custom_call" | custom-call | tf_op jit(solution)/shard_map/mixer/pallas_call | solution.py:643
  91.6 2.1 %copy.15 = bf16[768,512]{1,0:T(8,128)(2,1)} copy(bf16[768,512]{1,0:T(8,128)(2,1)} %mixer.1) | data formatting | bytes 1572864
  (2 shorter events, 0.0 us)

commit v7 on v6

--- a/solution.py
+++ b/solution.py
@@ -27,7 +27,7 @@
     out_ref,
     hid, wp, k_own, v_own, q_src, lam_in, gated, halo, u_b,
     k_all, v_all, q_own, qa, lam_own, s0, s1, s2, acc, m_ref, o_stage,
-    act, wtc, wta, sbuf, rbuf, mixc, mix, stats,
+    act, wtc, wta, sbuf, rbuf, mixc, total_mix, mix, stats,
     h_sem, w_sem, ow_sem, ow_send, ow_recv, aw_sem, aw_send, aw_recv, zw_send, zw_recv, halo_send, halo_recv,
     k_recv, v_recv, q_recv, l_recv, o_recv,
     q_send, l_send, p1k_send, p1v_send, rk_send, rv_send, lk_send, lv_send,
@@ -307,9 +307,9 @@
         return carry
 
     lax.fori_loop(0, NT, inner_rows, 0)
-    start_rest(*k_ring)
     loads[7].wait()
     lax.fori_loop(0, NT, gated_rows, 0)
+    start_rest(*k_ring)
     loads[8].wait()
 
     def gate_rows(m, carry):
@@ -479,7 +479,11 @@
         u = jnp.where(w == 3, last, plain)
         blk = block_of(w, u)
 
-        @pl.when((k == 3) & (w < 3))
+        @pl.when(i == 4)
+        def _():
+            exchange(1)
+
+        @pl.when((k == 3) & (0 < w) & (w < 3))
         def _():
             exchange(w + 1)
 
@@ -493,7 +497,7 @@
                 pair_out[4 + n].wait_recv()
                 zcopies[n].start()
 
-        for s, when in enumerate((1, 7, 12)):
+        for s, when in enumerate((1, 8, 14)):
 
             @pl.when(i == when)
             def _():
@@ -527,8 +531,6 @@
     lax.fori_loop(0, NB, step, 0)
 
     finish(1)
-
-    conv_ring(3)
 
     def piece(head):
         return act.at[4 + head]
@@ -557,25 +559,49 @@
     pass_on(mine[0], down)
     pass_on(mine[0], beside)
     pass_on(mine[1], beside)
+
+    for one in zcopies:
+        one.wait_recv()
+
+    def add_plane(n):
+        plane = (y + n) % 4
+        weights = wta[pl.ds(plane * 2, 2)].reshape(512, 512)
+        for r in range(3):
+            at = slice(r * TQ, (r + 1) * TQ)
+            rows = jnp.concatenate([act[4 + plane * 4 + h, at, :] for h in range(4)], axis=1)
+            part = jnp.dot(rows, weights, preferred_element_type=F32)
+            if n == 0:
+                total_mix[at, :] = part
+            elif n != 2:
+                total_mix[at, :] += part
+            else:
+                part = part + total_mix[at, :] + mixc[at, :]
+                mix[at, :] = part.astype(BF16)
+
+    def from_partner(n):
+        for e in range(2):
+            o_arrived(((y + n) % 4) * 4 + 2 * (1 - c) + e)
+
+    from_partner(0)
+    add_plane(0)
     o_arrived(below[0])
     pass_on(below[0], up)
     o_arrived(above[1])
     pass_on(above[1], down)
     pass_on(below[0], beside)
     pass_on(above[1], beside)
-    for head in (below[1], above[0], across[0], across[1]):
+    conv_ring(3)
+    for head in (below[1], above[0]):
         o_arrived(head)
         pass_on(head, beside)
-    for one in zcopies:
-        one.wait_recv()
-    for n in (0, 1, 3, 2):
-        for e in range(2):
-            o_arrived(((y + n) % 4) * 4 + 2 * (1 - c) + e)
-    for n in range(4):
-        first = n * PR
-        rows = jnp.concatenate([act[4 + h, first : first + PR, :] for h in range(16)], axis=1)
-        part = jnp.dot(rows, wta[...].reshape(2048, 512), preferred_element_type=F32)
-        mix[first : first + PR, :] = (part + mixc[first : first + PR, :]).astype(BF16)
+    for n in (3, 1):
+        from_partner(n)
+        add_plane(n)
+    for head in across:
+        o_arrived(head)
+        pass_on(head, beside)
+    from_partner(2)
+    add_plane(2)
 
     ones_row = jnp.ones((8, 512), BF16)
     dims = (((1,), (1,)), ((), ()))
@@ -672,6 +698,7 @@
             pltpu.VMEM((3, 2, HALF, 512), BF16),
             pltpu.VMEM((3, 2, HALF, 512), BF16),
             pltpu.VMEM((TB, 512), F32),
+            pltpu.VMEM((TB, 512), F32),
             pltpu.VMEM((TB, 512), BF16),
             pltpu.VMEM((8, 8, TB), F32),
             dma((NT,)), dma((6,)), dma((4,)), dma((4,)), dma((4,)), dma, dma((7,)), dma((7,)), dma((7,)), dma((7,)), dma, dma,

time: 94.9 us -> 92.1 us (0.970); the launches traced: 93.7 us -> 92 us
  Pallas kernels: 90.4 us -> 88.8 us
    pallas_call x1, Pallas kernels: 90.4 us -> 88.8 us  [mixer(): pl.pallas_call(mixer_kernel, out_shape=jax.ShapeDtypeStruct((TB, 512), BF...]
where the time goes in v7:
time: 92.1 us; the launch traced here: 92 us
  Pallas kernels  88.8 us (96%)
  local copies, waits for them, and re-layouts  2.06 us (2%)
  other arithmetic  1.13 us (1%)
    pallas_call x1, Pallas kernels, mixer(): pl.pallas_call(mixer_kernel, out_shape=jax.ShapeDtypeStruct((TB, 512), BF...  88.8 us
    unnamed x1, local copies, waits for them, and re-layouts  2.06 us

profile of v7, /device:TPU:1, one launch (start us, length us, event | category | flops | bytes accessed | tf_op | source)
XLA Modules:
  0.0 92.0 jit_solution(15583815001163699442)
XLA Ops:
  0.0 0.4 multiply_cosine_fusion
  0.4 0.7 pad_maximum_fusion.cs_ref
  1.1 88.8 %mixer.1 = bf16[768,512]{1,0:T(8,128)(2,1)} custom-call(bf16[768,4096]{1,0:T(8,128)(2,1)} %hid_in.1, bf16[4096,256]{1,0:T(8,128)(2,1)} %wk_in.1, bf16[4096,256]{1,0:T(8,128)(2,1)} %wv_in.1, bf16[4096,256]{1,0:T(8,128)(2,1)} %wq_in.1, bf16[4096,256]{1,0:T(8,128)(2,1)} %wb_in.1, bf16[4096,256]{1,0:T(8,128)(2,1)} %wc_in.1, bf16[4096,256]{1,0:T(8,128)(2,1)} %wh_in.1, ...), custom_call_target="tpu_custom_call" | custom-call | tf_op jit(solution)/shard_map/mixer/pallas_call | solution.py:669
  89.9 2.1 %copy.15 = bf16[768,512]{1,0:T(8,128)(2,1)} copy(bf16[768,512]{1,0:T(8,128)(2,1)} %mixer.1) | data formatting | bytes 1572864
  (2 shorter events, 0.0 us)

commit v8 on v7

--- a/solution.py
+++ b/solution.py
@@ -368,12 +368,10 @@
             )
             m_ref[at] = after
 
-        produce(0)
-        produce(1)
-        consume(0)
-        produce(2)
-        consume(1)
-        consume(2)
+        for t in range(NT):
+            produce(t)
+        for t in range(NT):
+            consume(t)
 
     def exchange(w):
         from_left, from_right = block_of(w, c), block_of(w, c + 2)

time: 92.1 us -> 91.4 us (level)
  no operation moved by 1% of the time
where the time goes in v8:
time: 91.4 us; the launch traced here: 91.3 us
  Pallas kernels  88.1 us (96%)
  local copies, waits for them, and re-layouts  2.06 us (2%)
  other arithmetic  1.13 us (1%)
    pallas_call x1, Pallas kernels, mixer(): pl.pallas_call(mixer_kernel, out_shape=jax.ShapeDtypeStruct((TB, 512), BF...  88.1 us
    unnamed x1, local copies, waits for them, and re-layouts  2.06 us

profile of v8, /device:TPU:1, one launch (start us, length us, event | category | flops | bytes accessed | tf_op | source)
XLA Modules:
  0.0 91.3 jit_solution(11494871836038982928)
XLA Ops:
  0.0 0.4 multiply_cosine_fusion
  0.4 0.7 pad_maximum_fusion.cs_ref
  1.1 88.1 %mixer.1 = bf16[768,512]{1,0:T(8,128)(2,1)} custom-call(bf16[768,4096]{1,0:T(8,128)(2,1)} %hid_in.1, bf16[4096,256]{1,0:T(8,128)(2,1)} %wk_in.1, bf16[4096,256]{1,0:T(8,128)(2,1)} %wv_in.1, bf16[4096,256]{1,0:T(8,128)(2,1)} %wq_in.1, bf16[4096,256]{1,0:T(8,128)(2,1)} %wb_in.1, bf16[4096,256]{1,0:T(8,128)(2,1)} %wc_in.1, bf16[4096,256]{1,0:T(8,128)(2,1)} %wh_in.1, ...), custom_call_target="tpu_custom_call" | custom-call | tf_op jit(solution)/shard_map/mixer/pallas_call | solution.py:667
  89.2 2.1 %copy.15 = bf16[768,512]{1,0:T(8,128)(2,1)} copy(bf16[768,512]{1,0:T(8,128)(2,1)} %mixer.1) | data formatting | bytes 1572864
  (2 shorter events, 0.0 us)
